TPU v7x, 32 devices: a whole 2x2x4 slice. The times are simulated.
32 devices in a mesh: kv: 16 (over z, y, core), tp: 2 (over x).
Axes of the slice: x: 2, y: 2, z: 4, core: 2. Of those that a mesh axis runs over, the one named last changes fastest.
Arguments:
- layer_input: bfloat16 [3072, 2048], P('kv', 'tp'), may hold values from -0.15625 to 0.15625
- queries: bfloat16 [3072, 1024], P('kv', 'tp'), may hold values from -6 to 6
- keys: bfloat16 [3072, 256], P('kv', 'tp'), may hold values from -6 to 6
- values: bfloat16 [3072, 256], P('kv', 'tp'), may hold values from -6 to 6
- attn_out: bfloat16 [3072, 1024], P('kv', 'tp'), may hold values from -1.25 to 1.25
- grad_out: bfloat16 [3072, 1024], P('kv', 'tp'), may hold values from -128 to 128
- log_sum: float32 [3072, 16], P('kv', 'tp'), may hold values from 6 to 7.5
- chosen: int32 [48, 8], replicated, may hold values from -1 to 47, as said below
Outputs:
- grad_queries: bfloat16 [3072, 1024], P('kv', 'tp')
- grad_keys: bfloat16 [3072, 256], P('kv', 'tp')
- grad_values: bfloat16 [3072, 256], P('kv', 'tp')
- grad_weight: float32 [2048, 1024], P('kv', 'tp')
Inputs may be any that keep to these rules, and one draw needn't show every extreme that they name: Write R = 3 and call positions [s * 192, (s + 1) * 192) segment s. For query block b in segment c = b // R and level l < 4, the entries chosen[b, 2 l + i] for i < 2 name 2 different key blocks of segment c - g_l, with g = 1, 2, 4, 8; all of them are -1 where c - g_l is negative.
All inputs are finite; a program needn't handle non-finite values.
Results may differ from a plain program's by a relative error of at most 0.0053.
Values may be sent and summed in bfloat16 or wider, within the bound.
A program may use at most 64 MiB of HBM per device.

v0:
```python
import functools
import math

import jax
import jax.numpy as jnp
from jax import lax
from jax.experimental import pallas as pl
from jax.experimental.pallas import tpu as pltpu
from jax.sharding import PartitionSpec as P

DH = 64
BLOCK = 64
PER = 2
LEVELS = 4
LOG2E = 1.4426950408889634
NEG = -1e30
NT = (((1,), (1,)), ((), ()))
TN = (((0,), (0,)), ((), ()))
NN = (((1,), (0,)), ((), ()))
BF = jnp.bfloat16
F32 = jnp.float32


def dot(a, b, dims):
    return lax.dot_general(a, b, dims, preferred_element_type=F32)


def kernel(cfg, *refs):
    n, tp, with_dw = cfg
    count_in = 7 if with_dw else 6
    hbm, refs = refs[:count_in], refs[count_in:]
    ch_ref, refs = refs[0], refs[1:]
    count_out = 4 if with_dw else 3
    outs, refs = refs[:count_out], refs[count_out:]
    held, refs = refs[:count_in], refs[count_in:]
    (in_s, qs, gs, lrow, drow, dqt, acc, kvbuf, gsend, grecv,
     kv_s, kv_r, g_s, g_r) = refs[:14]
    dq_out, dk_out, dv_out = outs[:3]
    k_ref, v_ref, q_ref, g_ref, o_ref, lse_ref = held[:3] + held[-3:]
    if with_dw:
        x_ref = held[3]
        dw_out = outs[3]
        (xbuf, xt, dqall, part, precv, x_s, x_r, a_s, a_r, f_s, f_r, w_s, w_r) = refs[14:]
    loads = [pltpu.make_async_copy(hbm[i], held[i], in_s.at[i]) for i in range(count_in)]
    for load in loads:
        load.start()
    me = lax.axis_index("kv")
    mt = lax.axis_index("tp")
    tok = q_ref.shape[0]
    kvh = k_ref.shape[1] // DH
    qh = q_ref.shape[1] // DH
    grp = qh // kvh
    nb = tok // BLOCK
    cols = grp * tok
    scale = DH ** -0.5
    dist = [1, n // 8, n // 4, n // 2]
    if with_dw:
        wn = math.isqrt(n)
        zn = n // wn
        zper = zn // tp
        rows = dw_out.shape[0]
        z = me // wn
        w = lax.rem(me, wn)
        plane = []
        for dw_ in range(wn):
            for dt in range(tp):
                if dw_ or dt:
                    plane.append((dw_, dt))

    def peer(dw_, dt):
        return {"kv": z * wn + lax.rem(w + dw_, wn), "tp": lax.rem(mt + dt, tp)}

    barrier = pltpu.get_barrier_semaphore()
    count = jnp.int32(0)
    for d in dist:
        @pl.when(me + d < n)
        def _():
            pl.semaphore_signal(barrier, inc=1, device_id={"kv": me + d}, device_id_type=pl.DeviceIdType.MESH)

        @pl.when(me >= d)
        def _():
            pl.semaphore_signal(barrier, inc=1, device_id={"kv": me - d}, device_id_type=pl.DeviceIdType.MESH)

        count = count + jnp.where(me + d < n, 1, 0) + jnp.where(me >= d, 1, 0)
    if with_dw:
        for dw_, dt in plane:
            pl.semaphore_signal(barrier, inc=1, device_id=peer(dw_, dt), device_id_type=pl.DeviceIdType.MESH)
        for s in range(1, zn):
            pl.semaphore_signal(barrier, inc=1, device_id={"kv": lax.rem(z + s, zn) * wn + w}, device_id_type=pl.DeviceIdType.MESH)
        count = count + len(plane) + zn - 1
    pl.semaphore_wait(barrier, count)

    def kv_copy(level, i):
        return pltpu.make_async_remote_copy(
            src_ref=(k_ref, v_ref)[i], dst_ref=kvbuf.at[level, i],
            send_sem=kv_s.at[level, i], recv_sem=kv_r.at[level, i],
            device_id={"kv": me + dist[level]}, device_id_type=pl.DeviceIdType.MESH)

    def g_copy(level):
        return pltpu.make_async_remote_copy(
            src_ref=gsend.at[level], dst_ref=grecv.at[level],
            send_sem=g_s.at[level], recv_sem=g_r.at[level],
            device_id={"kv": me - dist[level]}, device_id_type=pl.DeviceIdType.MESH)

    loads[0].wait()
    loads[1].wait()
    turns = [0, 1, 3, 2]
    for level in turns:
        @pl.when(me + dist[level] < n)
        def _():
            kv_copy(level, 0).start()
            kv_copy(level, 1).start()

    if with_dw:
        def x_copy(idx, zz):
            dw_, dt = plane[idx]
            wt = lax.rem(w + dw_, wn)
            off = pl.multiple_of((zz * wn + wt) * rows, rows)
            return pltpu.make_async_remote_copy(
                src_ref=x_ref.at[:, pl.ds(off, rows)],
                dst_ref=xbuf.at[mt * zper + zz, pl.ds(pl.multiple_of(w * tok, tok), tok)],
                send_sem=x_s.at[idx, zz], recv_sem=x_r.at[idx, zz],
                device_id=peer(dw_, dt), device_id_type=pl.DeviceIdType.MESH)

        loads[3].wait()
        for idx in range(len(plane)):
            for zz in range(zper):
                x_copy(idx, zz).start()
        for zz in range(zper):
            off = pl.multiple_of((zz * wn + w) * rows, rows)
            xbuf[mt * zper + zz, pl.ds(pl.multiple_of(w * tok, tok), tok), :] = x_ref[:, pl.ds(off, rows)]

    for i in range(count_in):
        if i not in (0, 1, 3) or (i == 3 and not with_dw):
            loads[i].wait()
    lse_t = lse_ref[...] * (-LOG2E)
    prod = g_ref[...].astype(F32) * o_ref[...].astype(F32)
    hi = prod.astype(BF)
    lo = (prod - hi.astype(F32)).astype(BF)
    pick = (lax.broadcasted_iota(jnp.int32, (16, qh * DH), 1) // DH
            == lax.broadcasted_iota(jnp.int32, (16, qh * DH), 0)).astype(F32).astype(BF)
    delta_t = dot(pick, hi, NT) + dot(pick, lo, NT)
    for h in range(kvh):
        for g in range(grp):
            i = h * grp + g
            lrow[h, 0:1, g * tok:(g + 1) * tok] = lse_t[i:i + 1, 0:tok]
            drow[h, 0:1, g * tok:(g + 1) * tok] = delta_t[i:i + 1, :]
            qs[h, g * tok:(g + 1) * tok, :] = q_ref[:, i * DH:(i + 1) * DH]
            gs[h, g * tok:(g + 1) * tok, :] = g_ref[:, i * DH:(i + 1) * DH]

    q_block = lax.rem(lax.broadcasted_iota(jnp.int32, (1, cols), 1), tok) // BLOCK

    def run_pass(h, k, v, bias):
        lse = lrow[h, 0:1, :]
        st = dot(k, qs[h], NT) * (scale * LOG2E)
        if bias is None:
            kp = lax.broadcasted_iota(jnp.int32, (tok, cols), 0)
            qp = lax.rem(lax.broadcasted_iota(jnp.int32, (tok, cols), 1), tok)
            keep = (qp >= kp) & ((qp // BLOCK) == (kp // BLOCK))
            p = jnp.exp2(jnp.where(keep, st + lse, NEG))
        else:
            p = jnp.concatenate(
                [jnp.exp2(st[b * BLOCK:(b + 1) * BLOCK] + (lse + bias[b])) for b in range(nb)], axis=0)
        dp = dot(v, gs[h], NT)
        ds = (p * (dp - drow[h, 0:1, :])).astype(BF)
        dv = dot(p.astype(BF), gs[h], NN)
        dk = dot(ds, qs[h], NN) * scale
        dq = dot(k, ds, TN)
        return dq, dk, dv

    for h in range(kvh):
        lanes = slice(h * DH, (h + 1) * DH)
        dq, dk, dv = run_pass(h, k_ref[:, lanes], v_ref[:, lanes], None)
        dqt[h] = dq
        acc[0, :, lanes] = dk
        acc[1, :, lanes] = dv

    def level_bias(level):
        bias = []
        for kb in range(nb):
            row = jnp.full((1, cols), NEG, F32)
            target = (me - dist[level]) * nb + kb
            for qb in range(nb):
                hit = jnp.float32(NEG)
                for i in range(PER):
                    hit = jnp.where(ch_ref[PER * level + i, me * nb + qb] == target, jnp.float32(0.0), hit)
                row = jnp.where(q_block == qb, hit, row)
            bias.append(row)
        return bias

    def far_pass(level, h, bias):
        lanes = slice(h * DH, (h + 1) * DH)
        dq, dk, dv = run_pass(h, kvbuf[level, 0, :, lanes], kvbuf[level, 1, :, lanes], bias)
        dqt[h] = dqt[h] + dq
        gsend[level, 0, :, lanes] = dk.astype(BF)
        gsend[level, 1, :, lanes] = dv.astype(BF)

    for level in turns[:-1]:
        @pl.when(me >= dist[level])
        def _():
            kv_copy(level, 0).wait_recv()
            kv_copy(level, 1).wait_recv()
            bias = level_bias(level)
            for h in range(kvh):
                far_pass(level, h, bias)
            g_copy(level).start()

    if with_dw:
        mine = pl.ds(pl.multiple_of(w * tok, tok), tok)
        pair = w + 1 - 2 * lax.rem(w, 2)
        hops = list(range(2, wn, 2))

        def a_copy(h, s):
            to = pair if s == 0 else lax.rem(w + s, wn)
            return pltpu.make_async_remote_copy(
                src_ref=dqall.at[h, mine], dst_ref=dqall.at[h, mine],
                send_sem=a_s.at[h, s // 2], recv_sem=a_r.at[h, s // 2],
                device_id={"kv": z * wn + to}, device_id_type=pl.DeviceIdType.MESH)

        def f_copy(h, s):
            slot = pl.ds(pl.multiple_of(lax.rem(w + wn - s, wn) * tok, tok), tok)
            return pltpu.make_async_remote_copy(
                src_ref=dqall.at[h, slot], dst_ref=dqall.at[h, slot],
                send_sem=f_s.at[h, s // 2 - 1], recv_sem=f_r.at[h, s // 2 - 1],
                device_id={"kv": z * wn + pair}, device_id_type=pl.DeviceIdType.MESH)

    last = turns[-1]
    for h in range(kvh):
        @pl.when(me >= dist[last])
        def _():
            if h == 0:
                kv_copy(last, 0).wait_recv()
                kv_copy(last, 1).wait_recv()
            far_pass(last, h, level_bias(last))
        whole = dqt[h] * scale
        for g in range(grp):
            low = whole[:, g * tok:(g + 1) * tok].T.astype(BF)
            i = h * grp + g
            dq_out[:, i * DH:(i + 1) * DH] = low
            if with_dw:
                dqall[h, mine, g * DH:(g + 1) * DH] = low
        if with_dw:
            for s in hops:
                a_copy(h, s).start()
            a_copy(h, 0).start()

    @pl.when(me >= dist[last])
    def _():
        g_copy(last).start()

    if with_dw:
        for idx in range(len(plane)):
            for zz in range(zper):
                x_copy(idx, zz).wait()
        for zz in range(zn):
            xt[zz] = xbuf[zz].T

        near = z + 1 - 2 * lax.rem(z, 2)
        far = lax.rem(z + 2, zn)

        def w_copy(h, i):
            return pltpu.make_async_remote_copy(
                src_ref=part.at[h, i], dst_ref=precv.at[h, i],
                send_sem=w_s.at[h, i], recv_sem=w_r.at[h, i],
                device_id={"kv": (far if i == 2 else near) * wn + w}, device_id_type=pl.DeviceIdType.MESH)

        def send_near(h):
            part[h, 1] = dot(xt[near], dqall[h], NN).astype(BF)
            w_copy(h, 1).start()

        for h in range(kvh):
            for s in hops:
                a_copy(h, s).wait_recv()
                f_copy(h, s).start()
            a_copy(h, 0).wait_recv()
            for s in hops:
                f_copy(h, s).wait_recv()
            part[h, 0] = dot(xt[lax.rem(near + 2, zn)], dqall[h], NN).astype(BF)
            w_copy(h, 0).start()
        send_near(0)
        for h in range(kvh):
            ours = dot(xt[far], dqall[h], NN)
            w_copy(h, 0).wait_recv()
            part[h, 2] = (ours + precv[h, 0].astype(F32)).astype(BF)
            w_copy(h, 2).start()
        for h in range(1, kvh):
            send_near(h)
        width = grp * DH
        for h in range(kvh):
            dw_out[:, h * width:(h + 1) * width] = dot(xt[z], dqall[h], NN)
        for h in range(kvh):
            for s in [0] + hops:
                a_copy(h, s).wait_send()
            for s in hops:
                f_copy(h, s).wait_send()

    for level, d in enumerate(dist):
        @pl.when(me + d < n)
        def _():
            kv_copy(level, 0).wait_send()
            kv_copy(level, 1).wait_send()
            g_copy(level).wait_recv()
            acc[...] = acc[...] + grecv[level].astype(F32)

        @pl.when(me >= d)
        def _():
            g_copy(level).wait_send()

    dk_out[...] = acc[0].astype(BF)
    dv_out[...] = acc[1].astype(BF)
    if with_dw:
        for h in range(kvh):
            lanes = slice(h * width, (h + 1) * width)
            w_copy(h, 0).wait_send()
            w_copy(h, 1).wait()
            w_copy(h, 2).wait()
            dw_out[:, lanes] = dw_out[:, lanes] + precv[h, 1].astype(F32) + precv[h, 2].astype(F32)


def writer(*refs):
    count = (len(refs) - 1) // 2
    sem = refs[-1]
    copies = [pltpu.make_async_copy(refs[i], refs[count + i], sem.at[i]) for i in range(count)]
    for copy in copies:
        copy.start()
    for copy in copies:
        copy.wait()


def shards(layer_input, queries, keys, values, attn_out, grad_out, log_sum, chosen):
    n = lax.axis_size("kv")
    tp = lax.axis_size("tp")
    tok, qw = queries.shape
    kw = keys.shape[1]
    kvh, qh = kw // DH, qw // DH
    cols = qh // kvh * tok
    depth = layer_input.shape[1] * tp
    rows = depth // n
    wn = math.isqrt(n)
    zn = n // wn
    with_dw = wn * wn == n and zn == 4 and zn % tp == 0 and rows % 128 == 0
    vm = pl.BlockSpec(memory_space=pltpu.VMEM)
    out_shape = [
        jax.ShapeDtypeStruct((tok, qw), BF),
        jax.ShapeDtypeStruct((tok, kw), BF),
        jax.ShapeDtypeStruct((tok, kw), BF),
    ]
    args = [keys, values, queries, grad_out, attn_out, log_sum.T]
    if with_dw:
        args.insert(3, layer_input)
    scratch = [pltpu.VMEM(a.shape, a.dtype) for a in args] + [
        pltpu.SemaphoreType.DMA((len(args),)),
        pltpu.VMEM((kvh, cols, DH), BF),
        pltpu.VMEM((kvh, cols, DH), BF),
        pltpu.VMEM((kvh, 1, cols), F32),
        pltpu.VMEM((kvh, 1, cols), F32),
        pltpu.VMEM((kvh, DH, cols), F32),
        pltpu.VMEM((2, tok, kw), F32),
        pltpu.VMEM((LEVELS, 2, tok, kw), BF),
        pltpu.VMEM((LEVELS, 2, tok, kw), BF),
        pltpu.VMEM((LEVELS, 2, tok, kw), BF),
        pltpu.SemaphoreType.DMA((LEVELS, 2)),
        pltpu.SemaphoreType.DMA((LEVELS, 2)),
        pltpu.SemaphoreType.DMA((LEVELS,)),
        pltpu.SemaphoreType.DMA((LEVELS,)),
    ]
    hbm = pl.BlockSpec(memory_space=pltpu.HBM)
    specs = [hbm] * len(args) + [pl.BlockSpec(memory_space=pltpu.SMEM)]
    if with_dw:
        out_shape.append(jax.ShapeDtypeStruct((rows, qw), F32))
        peers = wn * tp - 1
        zper = zn // tp
        scratch += [
            pltpu.VMEM((zn, wn * tok, rows), BF),
            pltpu.VMEM((zn, rows, wn * tok), BF),
            pltpu.VMEM((kvh, wn * tok, qw // kvh), BF),
            pltpu.VMEM((kvh, zn - 1, rows, qw // kvh), BF),
            pltpu.VMEM((kvh, zn - 1, rows, qw // kvh), BF),
            pltpu.SemaphoreType.DMA((peers, zper)),
            pltpu.SemaphoreType.DMA((peers, zper)),
            pltpu.SemaphoreType.DMA((kvh, wn // 2)),
            pltpu.SemaphoreType.DMA((kvh, wn // 2)),
            pltpu.SemaphoreType.DMA((kvh, max(wn // 2 - 1, 1))),
            pltpu.SemaphoreType.DMA((kvh, max(wn // 2 - 1, 1))),
            pltpu.SemaphoreType.DMA((kvh, zn - 1)),
            pltpu.SemaphoreType.DMA((kvh, zn - 1)),
        ]
    outs = pl.pallas_call(
        functools.partial(kernel, (n, tp, with_dw)),
        out_shape=[pltpu.VMEM(a.shape, a.dtype) for a in out_shape],
        in_specs=specs,
        out_specs=[vm] * len(out_shape),
        scratch_shapes=scratch,
        compiler_params=pltpu.CompilerParams(
            collective_id=0, has_side_effects=True, vmem_limit_bytes=66100000),
    )(*args, chosen.T)
    outs = pl.pallas_call(
        writer,
        out_shape=out_shape,
        in_specs=[vm] * len(out_shape),
        out_specs=[hbm] * len(out_shape),
        scratch_shapes=[pltpu.SemaphoreType.DMA((len(out_shape),))],
        compiler_params=pltpu.CompilerParams(vmem_limit_bytes=1024 * 1024),
    )(*outs)
    if with_dw:
        return tuple(outs)
    whole_input = lax.all_gather(layer_input, "tp", axis=1, tiled=True)
    grad_weight = lax.psum_scatter(
        jnp.einsum("td,tc->dc", whole_input, outs[0], preferred_element_type=F32),
        "kv", scatter_dimension=0, tiled=True)
    return tuple(outs) + (grad_weight,)


def solution(mesh):
    spec = P("kv", "tp")
    return jax.shard_map(
        shards,
        mesh=mesh,
        in_specs=(spec,) * 7 + (P(),),
        out_specs=(spec,) * 4,
        check_vma=False,
    )
```

profile of v0, /device:TPU:0, one launch (start us, length us, event | category | flops | bytes accessed | tf_op | source)
XLA Modules:
  0.0 40.3 jit_solution(3903541686229500080)
XLA Ops:
  0.6 38.8 %shard_map.111 = (bf16[192,512]{1,0:T(8,128)(2,1)S(1)}, bf16[192,128]{1,0:T(8,128)(2,1)S(1)}, bf16[192,128]{1,0:T(8,128)(2,1)S(1)}, f32[128,512]{1,0:T(8,128)S(1)}) custom-call(bf16[192,128]{1,0:T(8,128)(2,1)} %refs_0_.1, bf16[192,128]{1,0:T(8,128)(2,1)} %refs_1_.1, bf16[192,512]{1,0:T(8,128)(2,1)} %refs_2_.1, bf16[192,1024]{1,0:T(8,128)(2,1)} %refs_3_.1, ...), custom_call_target="tpu_custom_call" | custom-call | tf_op jit(solution)/shard_map/pallas_call | solution.py:388
  39.4 0.8 %shard_map.112 = (bf16[192,512]{1,0:T(8,128)(2,1)}, bf16[192,128]{1,0:T(8,128)(2,1)}, bf16[192,128]{1,0:T(8,128)(2,1)}, f32[128,512]{1,0:T(8,128)}) custom-call(bf16[192,512]{1,0:T(8,128)(2,1)S(1)} %get-tuple-element.8.refs_0_, bf16[192,128]{1,0:T(8,128)(2,1)S(1)} %get-tuple-element.9.refs_1_, bf16[192,128]{1,0:T(8,128)(2,1)S(1)} %get-tuple-element.10.refs_2_, ...), custom_call_target="tpu_custom_call" | custom-call | tf_op jit(solution)/shard_map/pallas_call | solution.py:397
where the time goes:
time: 40.4 us; the launch traced here: 40.3 us
  Pallas kernels  39.6 us (98%)
  between operations  0.64 us (2%)
    pallas_call x1, Pallas kernels, shards(): pl.pallas_call(functools.partial(kernel, (n, tp, with_dw)), out_shape=[pl...  38.8 us
    pallas_call x1, Pallas kernels, shards(): pl.pallas_call(writer, out_shape=out_shape, in_specs=[vm] * len(out_shape...  0.84 us

commit v1 on v0

--- a/solution.py
+++ b/solution.py
@@ -29,10 +29,11 @@
     n, tp, with_dw = cfg
     count_in = 7 if with_dw else 6
     hbm, refs = refs[:count_in], refs[count_in:]
-    ch_ref, refs = refs[0], refs[1:]
+    ch_hbm, refs = refs[0], refs[1:]
     count_out = 4 if with_dw else 3
     outs, refs = refs[:count_out], refs[count_out:]
     held, refs = refs[:count_in], refs[count_in:]
+    ch_ref, refs = refs[0], refs[1:]
     (in_s, qs, gs, lrow, drow, dqt, acc, kvbuf, gsend, grecv,
      kv_s, kv_r, g_s, g_r) = refs[:14]
     dq_out, dk_out, dv_out = outs[:3]
@@ -42,6 +43,7 @@
         dw_out = outs[3]
         (xbuf, xt, dqall, part, precv, x_s, x_r, a_s, a_r, f_s, f_r, w_s, w_r) = refs[14:]
     loads = [pltpu.make_async_copy(hbm[i], held[i], in_s.at[i]) for i in range(count_in)]
+    loads.append(pltpu.make_async_copy(ch_hbm, ch_ref, in_s.at[count_in]))
     for load in loads:
         load.start()
     me = lax.axis_index("kv")
@@ -61,14 +63,12 @@
         rows = dw_out.shape[0]
         z = me // wn
         w = lax.rem(me, wn)
-        plane = []
-        for dw_ in range(wn):
-            for dt in range(tp):
-                if dw_ or dt:
-                    plane.append((dw_, dt))
-
-    def peer(dw_, dt):
-        return {"kv": z * wn + lax.rem(w + dw_, wn), "tp": lax.rem(mt + dt, tp)}
+        pair = w + 1 - 2 * lax.rem(w, 2)
+        across = lax.rem(w + 2, wn)
+        across_pair = lax.rem(pair + 2, wn)
+        near = z + 1 - 2 * lax.rem(z, 2)
+        far = lax.rem(z + 2, zn)
+        plane = [(pair, mt), (across, mt), (across_pair, mt), (w, 1 - mt), (pair, 1 - mt)]
 
     barrier = pltpu.get_barrier_semaphore()
     count = jnp.int32(0)
@@ -83,11 +83,11 @@
 
         count = count + jnp.where(me + d < n, 1, 0) + jnp.where(me >= d, 1, 0)
     if with_dw:
-        for dw_, dt in plane:
-            pl.semaphore_signal(barrier, inc=1, device_id=peer(dw_, dt), device_id_type=pl.DeviceIdType.MESH)
-        for s in range(1, zn):
-            pl.semaphore_signal(barrier, inc=1, device_id={"kv": lax.rem(z + s, zn) * wn + w}, device_id_type=pl.DeviceIdType.MESH)
-        count = count + len(plane) + zn - 1
+        for wt, tt in plane:
+            pl.semaphore_signal(barrier, inc=1, device_id={"kv": z * wn + wt, "tp": tt}, device_id_type=pl.DeviceIdType.MESH)
+        for zt in (near, far):
+            pl.semaphore_signal(barrier, inc=1, device_id={"kv": zt * wn + w}, device_id_type=pl.DeviceIdType.MESH)
+        count = count + len(plane) + 2
     pl.semaphore_wait(barrier, count)
 
     def kv_copy(level, i):
@@ -113,24 +113,30 @@
 
     if with_dw:
         def x_copy(idx, zz):
-            dw_, dt = plane[idx]
-            wt = lax.rem(w + dw_, wn)
+            wt, tt = plane[idx]
             off = pl.multiple_of((zz * wn + wt) * rows, rows)
             return pltpu.make_async_remote_copy(
                 src_ref=x_ref.at[:, pl.ds(off, rows)],
                 dst_ref=xbuf.at[mt * zper + zz, pl.ds(pl.multiple_of(w * tok, tok), tok)],
                 send_sem=x_s.at[idx, zz], recv_sem=x_r.at[idx, zz],
-                device_id=peer(dw_, dt), device_id_type=pl.DeviceIdType.MESH)
+                device_id={"kv": z * wn + wt, "tp": tt}, device_id_type=pl.DeviceIdType.MESH)
+
+        def x_forward(idx, zz):
+            slot = xbuf.at[mt * zper + zz, pl.ds(pl.multiple_of(plane[idx][0] * tok, tok), tok)]
+            return pltpu.make_async_remote_copy(
+                src_ref=slot, dst_ref=slot,
+                send_sem=x_s.at[idx + 4, zz], recv_sem=x_r.at[idx + 4, zz],
+                device_id={"kv": me, "tp": 1 - mt}, device_id_type=pl.DeviceIdType.MESH)
 
         loads[3].wait()
-        for idx in range(len(plane)):
-            for zz in range(zper):
+        for zz in range(zper):
+            for idx in (1, 2, 3, 4, 0):
                 x_copy(idx, zz).start()
         for zz in range(zper):
             off = pl.multiple_of((zz * wn + w) * rows, rows)
             xbuf[mt * zper + zz, pl.ds(pl.multiple_of(w * tok, tok), tok), :] = x_ref[:, pl.ds(off, rows)]
 
-    for i in range(count_in):
+    for i in range(count_in + 1):
         if i not in (0, 1, 3) or (i == 3 and not with_dw):
             loads[i].wait()
     lse_t = lse_ref[...] * (-LOG2E)
@@ -207,7 +213,6 @@
 
     if with_dw:
         mine = pl.ds(pl.multiple_of(w * tok, tok), tok)
-        pair = w + 1 - 2 * lax.rem(w, 2)
         hops = list(range(2, wn, 2))
 
         def a_copy(h, s):
@@ -223,6 +228,12 @@
                 src_ref=dqall.at[h, slot], dst_ref=dqall.at[h, slot],
                 send_sem=f_s.at[h, s // 2 - 1], recv_sem=f_r.at[h, s // 2 - 1],
                 device_id={"kv": z * wn + pair}, device_id_type=pl.DeviceIdType.MESH)
+
+    if with_dw:
+        for zz in range(zper):
+            for idx in (1, 2):
+                x_copy(idx, zz).wait_recv()
+                x_forward(idx, zz).start()
 
     last = turns[-1]
     for h in range(kvh):
@@ -249,14 +260,15 @@
         g_copy(last).start()
 
     if with_dw:
-        for idx in range(len(plane)):
-            for zz in range(zper):
-                x_copy(idx, zz).wait()
+        for zz in range(zper):
+            for idx in range(len(plane)):
+                if idx in (1, 2):
+                    x_copy(idx, zz).wait_send()
+                    x_forward(idx, zz).wait()
+                else:
+                    x_copy(idx, zz).wait()
         for zz in range(zn):
             xt[zz] = xbuf[zz].T
-
-        near = z + 1 - 2 * lax.rem(z, 2)
-        far = lax.rem(z + 2, zn)
 
         def w_copy(h, i):
             return pltpu.make_async_remote_copy(
@@ -338,7 +350,7 @@
     rows = depth // n
     wn = math.isqrt(n)
     zn = n // wn
-    with_dw = wn * wn == n and zn == 4 and zn % tp == 0 and rows % 128 == 0
+    with_dw = wn * wn == n and zn == 4 and tp == 2 and rows % 128 == 0
     vm = pl.BlockSpec(memory_space=pltpu.VMEM)
     out_shape = [
         jax.ShapeDtypeStruct((tok, qw), BF),
@@ -349,7 +361,8 @@
     if with_dw:
         args.insert(3, layer_input)
     scratch = [pltpu.VMEM(a.shape, a.dtype) for a in args] + [
-        pltpu.SemaphoreType.DMA((len(args),)),
+        pltpu.SMEM(chosen.T.shape, chosen.dtype),
+        pltpu.SemaphoreType.DMA((len(args) + 1,)),
         pltpu.VMEM((kvh, cols, DH), BF),
         pltpu.VMEM((kvh, cols, DH), BF),
         pltpu.VMEM((kvh, 1, cols), F32),
@@ -365,10 +378,10 @@
         pltpu.SemaphoreType.DMA((LEVELS,)),
     ]
     hbm = pl.BlockSpec(memory_space=pltpu.HBM)
-    specs = [hbm] * len(args) + [pl.BlockSpec(memory_space=pltpu.SMEM)]
+    specs = [hbm] * (len(args) + 1)
     if with_dw:
         out_shape.append(jax.ShapeDtypeStruct((rows, qw), F32))
-        peers = wn * tp - 1
+        peers = 7
         zper = zn // tp
         scratch += [
             pltpu.VMEM((zn, wn * tok, rows), BF),

time: 40.4 us -> 35.5 us (0.88)
  Pallas kernels: 39.6 us -> 34.8 us
    pallas_call x1, Pallas kernels: 38.8 us -> 33.9 us  [shards(): pl.pallas_call(functools.partial(kernel, (n, tp, with_dw)), out_shape=[pl...]
where the time goes in v1:
time: 35.5 us; the launch traced here: 35.4 us
  Pallas kernels  34.8 us (98%)
  between operations  0.64 us (2%)
    pallas_call x1, Pallas kernels, shards(): pl.pallas_call(functools.partial(kernel, (n, tp, with_dw)), out_shape=[pl...  33.9 us
    pallas_call x1, Pallas kernels, shards(): pl.pallas_call(writer, out_shape=out_shape, in_specs=[vm] * len(out_shape...  0.84 us

profile of v1, /device:TPU:0, one launch (start us, length us, event | category | flops | bytes accessed | tf_op | source)
XLA Modules:
  0.0 35.4 jit_solution(7492760371359338216)
XLA Ops:
  0.6 33.9 %shard_map.111 = (bf16[192,512]{1,0:T(8,128)(2,1)S(1)}, bf16[192,128]{1,0:T(8,128)(2,1)S(1)}, bf16[192,128]{1,0:T(8,128)(2,1)S(1)}, f32[128,512]{1,0:T(8,128)S(1)}) custom-call(bf16[192,128]{1,0:T(8,128)(2,1)} %refs_0_.1, bf16[192,128]{1,0:T(8,128)(2,1)} %refs_1_.1, bf16[192,512]{1,0:T(8,128)(2,1)} %refs_2_.1, bf16[192,1024]{1,0:T(8,128)(2,1)} %refs_3_.1, ...), custom_call_target="tpu_custom_call" | custom-call | tf_op jit(solution)/shard_map/pallas_call | solution.py:401
  34.6 0.8 %shard_map.112 = (bf16[192,512]{1,0:T(8,128)(2,1)}, bf16[192,128]{1,0:T(8,128)(2,1)}, bf16[192,128]{1,0:T(8,128)(2,1)}, f32[128,512]{1,0:T(8,128)}) custom-call(bf16[192,512]{1,0:T(8,128)(2,1)S(1)} %get-tuple-element.8.refs_0_, bf16[192,128]{1,0:T(8,128)(2,1)S(1)} %get-tuple-element.9.refs_1_, bf16[192,128]{1,0:T(8,128)(2,1)S(1)} %get-tuple-element.10.refs_2_, ...), custom_call_target="tpu_custom_call" | custom-call | tf_op jit(solution)/shard_map/pallas_call | solution.py:410

commit v2 on v1

--- a/solution.py
+++ b/solution.py
@@ -56,6 +56,12 @@
     cols = grp * tok
     scale = DH ** -0.5
     dist = [1, n // 8, n // 4, n // 2]
+
+    def span(level):
+        if isinstance(level, int):
+            return dist[level]
+        return jnp.where(level == 0, dist[0], jnp.where(level == 1, dist[1], jnp.where(level == 2, dist[2], dist[3])))
+
     if with_dw:
         wn = math.isqrt(n)
         zn = n // wn
@@ -68,11 +74,15 @@
         across_pair = lax.rem(pair + 2, wn)
         near = z + 1 - 2 * lax.rem(z, 2)
         far = lax.rem(z + 2, zn)
+        partner = me + 1 - 2 * lax.rem(me, 2)
+        first = lax.rem(me, 2) == 0
+        second = lax.rem(me, 2) == 1
+        order = [1 - lax.rem(z, 2), lax.rem(z, 2)]
         plane = [(pair, mt), (across, mt), (across_pair, mt), (w, 1 - mt), (pair, 1 - mt)]
 
     barrier = pltpu.get_barrier_semaphore()
     count = jnp.int32(0)
-    for d in dist:
+    for d in dist[1:] if with_dw else dist:
         @pl.when(me + d < n)
         def _():
             pl.semaphore_signal(barrier, inc=1, device_id={"kv": me + d}, device_id_type=pl.DeviceIdType.MESH)
@@ -94,44 +104,62 @@
         return pltpu.make_async_remote_copy(
             src_ref=(k_ref, v_ref)[i], dst_ref=kvbuf.at[level, i],
             send_sem=kv_s.at[level, i], recv_sem=kv_r.at[level, i],
-            device_id={"kv": me + dist[level]}, device_id_type=pl.DeviceIdType.MESH)
+            device_id={"kv": me + span(level)}, device_id_type=pl.DeviceIdType.MESH)
+
+    def kv_pass_on(level, i, held_kv):
+        to, src = (0, held_kv) if level == 0 else (3, kvbuf.at[2, i])
+        return pltpu.make_async_remote_copy(
+            src_ref=src, dst_ref=kvbuf.at[to, i],
+            send_sem=kv_s.at[to, i], recv_sem=kv_r.at[to, i],
+            device_id={"kv": partner if level == 0 else me + dist[2]}, device_id_type=pl.DeviceIdType.MESH)
 
     def g_copy(level):
+        to = jnp.where(level == 0, partner, me - span(level)) if with_dw else me - dist[level]
         return pltpu.make_async_remote_copy(
             src_ref=gsend.at[level], dst_ref=grecv.at[level],
             send_sem=g_s.at[level], recv_sem=g_r.at[level],
-            device_id={"kv": me - dist[level]}, device_id_type=pl.DeviceIdType.MESH)
+            device_id={"kv": to}, device_id_type=pl.DeviceIdType.MESH)
 
     loads[0].wait()
     loads[1].wait()
     turns = [0, 1, 3, 2]
-    for level in turns:
+    if with_dw:
+        late = w == 0
+        turns = [jnp.where(second, 0, 2), jnp.where(second, 2, jnp.where(late, 0, 1)),
+                 jnp.where(second, 1, jnp.where(late, 3, 0)), jnp.where(late, 1, 3)]
+    for level in (2, 1) if with_dw else turns:
         @pl.when(me + dist[level] < n)
         def _():
             kv_copy(level, 0).start()
             kv_copy(level, 1).start()
 
     if with_dw:
-        def x_copy(idx, zz):
+        @pl.when(first)
+        def _():
+            kv_pass_on(0, 0, k_ref).start()
+            kv_pass_on(0, 1, v_ref).start()
+
+        def x_copy(idx, k):
             wt, tt = plane[idx]
+            zz = order[k]
             off = pl.multiple_of((zz * wn + wt) * rows, rows)
             return pltpu.make_async_remote_copy(
                 src_ref=x_ref.at[:, pl.ds(off, rows)],
                 dst_ref=xbuf.at[mt * zper + zz, pl.ds(pl.multiple_of(w * tok, tok), tok)],
-                send_sem=x_s.at[idx, zz], recv_sem=x_r.at[idx, zz],
+                send_sem=x_s.at[idx, k], recv_sem=x_r.at[idx, k],
                 device_id={"kv": z * wn + wt, "tp": tt}, device_id_type=pl.DeviceIdType.MESH)
 
-        def x_forward(idx, zz):
-            slot = xbuf.at[mt * zper + zz, pl.ds(pl.multiple_of(plane[idx][0] * tok, tok), tok)]
+        def x_forward(idx, k):
+            slot = xbuf.at[mt * zper + order[k], pl.ds(pl.multiple_of(plane[idx][0] * tok, tok), tok)]
             return pltpu.make_async_remote_copy(
                 src_ref=slot, dst_ref=slot,
-                send_sem=x_s.at[idx + 4, zz], recv_sem=x_r.at[idx + 4, zz],
+                send_sem=x_s.at[idx + 4, k], recv_sem=x_r.at[idx + 4, k],
                 device_id={"kv": me, "tp": 1 - mt}, device_id_type=pl.DeviceIdType.MESH)
 
         loads[3].wait()
-        for zz in range(zper):
+        for k in range(zper):
             for idx in (1, 2, 3, 4, 0):
-                x_copy(idx, zz).start()
+                x_copy(idx, k).start()
         for zz in range(zper):
             off = pl.multiple_of((zz * wn + w) * rows, rows)
             xbuf[mt * zper + zz, pl.ds(pl.multiple_of(w * tok, tok), tok), :] = x_ref[:, pl.ds(off, rows)]
@@ -185,7 +213,7 @@
         bias = []
         for kb in range(nb):
             row = jnp.full((1, cols), NEG, F32)
-            target = (me - dist[level]) * nb + kb
+            target = (me - span(level)) * nb + kb
             for qb in range(nb):
                 hit = jnp.float32(NEG)
                 for i in range(PER):
@@ -201,15 +229,52 @@
         gsend[level, 0, :, lanes] = dk.astype(BF)
         gsend[level, 1, :, lanes] = dv.astype(BF)
 
-    for level in turns[:-1]:
-        @pl.when(me >= dist[level])
-        def _():
-            kv_copy(level, 0).wait_recv()
-            kv_copy(level, 1).wait_recv()
-            bias = level_bias(level)
-            for h in range(kvh):
-                far_pass(level, h, bias)
+    def wait_kv(level):
+        kv_copy(level, 0).wait_recv()
+        kv_copy(level, 1).wait_recv()
+
+    def far_level(level):
+        bias = level_bias(level)
+        for h in range(kvh):
+            far_pass(level, h, bias)
+
+    def arrive(level):
+        wait_kv(level)
+        if with_dw:
+            @pl.when((level == 2) & (me + dist[2] < n))
+            def _():
+                kv_pass_on(3, 0, None).start()
+                kv_pass_on(3, 1, None).start()
+
+            @pl.when((level == 1) & second)
+            def _():
+                kv_pass_on(0, 0, kvbuf.at[1, 0]).start()
+                kv_pass_on(0, 1, kvbuf.at[1, 1]).start()
+
+    def return_level(level):
+        if with_dw:
+            @pl.when(level != 1)
+            def _():
+                g_copy(level).start()
+        else:
             g_copy(level).start()
+
+    def pass_x_on(k):
+        for idx in (1, 2):
+            x_copy(idx, k).wait_recv()
+            x_forward(idx, k).start()
+
+    for turn, level in enumerate(turns[:-1]):
+        if with_dw and turn == 2:
+            @pl.when((z >= 1) & first)
+            def _():
+                pass_x_on(0)
+
+        @pl.when(me >= span(level))
+        def _():
+            arrive(level)
+            far_level(level)
+            return_level(level)
 
     if with_dw:
         mine = pl.ds(pl.multiple_of(w * tok, tok), tok)
@@ -230,18 +295,16 @@
                 device_id={"kv": z * wn + pair}, device_id_type=pl.DeviceIdType.MESH)
 
     if with_dw:
-        for zz in range(zper):
-            for idx in (1, 2):
-                x_copy(idx, zz).wait_recv()
-                x_forward(idx, zz).start()
+        @pl.when((z >= 2) & second)
+        def _():
+            pass_x_on(0)
 
     last = turns[-1]
     for h in range(kvh):
-        @pl.when(me >= dist[last])
+        @pl.when(me >= span(last))
         def _():
             if h == 0:
-                kv_copy(last, 0).wait_recv()
-                kv_copy(last, 1).wait_recv()
+                arrive(last)
             far_pass(last, h, level_bias(last))
         whole = dqt[h] * scale
         for g in range(grp):
@@ -255,20 +318,34 @@
                 a_copy(h, s).start()
             a_copy(h, 0).start()
 
-    @pl.when(me >= dist[last])
+    @pl.when(me >= span(last))
     def _():
-        g_copy(last).start()
-
-    if with_dw:
-        for zz in range(zper):
-            for idx in range(len(plane)):
-                if idx in (1, 2):
-                    x_copy(idx, zz).wait_send()
-                    x_forward(idx, zz).wait()
-                else:
-                    x_copy(idx, zz).wait()
-        for zz in range(zn):
-            xt[zz] = xbuf[zz].T
+        return_level(last)
+
+    def early_sum():
+        @pl.when(second)
+        def _():
+            g_copy(0).wait_recv()
+            gsend[1] = (gsend[1].astype(F32) + grecv[0].astype(F32)).astype(BF)
+
+        g_copy(1).start()
+
+    if with_dw:
+        @pl.when((z < 1) | ((z < 2) & second))
+        def _():
+            pass_x_on(0)
+
+        pass_x_on(1)
+
+        @pl.when((me >= dist[1]) & (w < 2))
+        def _():
+            early_sum()
+
+        def x_arrive(k):
+            for idx in (0, 3, 4):
+                x_copy(idx, k).wait_recv()
+            for idx in (1, 2):
+                x_forward(idx, k).wait_recv()
 
         def w_copy(h, i):
             return pltpu.make_async_remote_copy(
@@ -276,47 +353,97 @@
                 send_sem=w_s.at[h, i], recv_sem=w_r.at[h, i],
                 device_id={"kv": (far if i == 2 else near) * wn + w}, device_id_type=pl.DeviceIdType.MESH)
 
-        def send_near(h):
-            part[h, 1] = dot(xt[near], dqall[h], NN).astype(BF)
-            w_copy(h, 1).start()
-
         for h in range(kvh):
             for s in hops:
                 a_copy(h, s).wait_recv()
                 f_copy(h, s).start()
+            if h == 0:
+                x_arrive(0)
+                for zz in (lax.rem(near + 2, zn), near):
+                    xt[zz] = xbuf[zz].T
             a_copy(h, 0).wait_recv()
             for s in hops:
                 f_copy(h, s).wait_recv()
             part[h, 0] = dot(xt[lax.rem(near + 2, zn)], dqall[h], NN).astype(BF)
             w_copy(h, 0).start()
-        send_near(0)
+            part[h, 1] = dot(xt[near], dqall[h], NN).astype(BF)
+            w_copy(h, 1).start()
+        @pl.when(w >= 2)
+        def _():
+            early_sum()
+
+        x_arrive(1)
+        for zz in (far, z):
+            xt[zz] = xbuf[zz].T
         for h in range(kvh):
             ours = dot(xt[far], dqall[h], NN)
             w_copy(h, 0).wait_recv()
             part[h, 2] = (ours + precv[h, 0].astype(F32)).astype(BF)
             w_copy(h, 2).start()
-        for h in range(1, kvh):
-            send_near(h)
         width = grp * DH
         for h in range(kvh):
             dw_out[:, h * width:(h + 1) * width] = dot(xt[z], dqall[h], NN)
+        for k in range(zper):
+            for idx in range(len(plane)):
+                x_copy(idx, k).wait_send()
+            for idx in (1, 2):
+                x_forward(idx, k).wait_send()
         for h in range(kvh):
             for s in [0] + hops:
                 a_copy(h, s).wait_send()
             for s in hops:
                 f_copy(h, s).wait_send()
 
-    for level, d in enumerate(dist):
-        @pl.when(me + d < n)
-        def _():
-            kv_copy(level, 0).wait_send()
-            kv_copy(level, 1).wait_send()
-            g_copy(level).wait_recv()
-            acc[...] = acc[...] + grecv[level].astype(F32)
-
-        @pl.when(me >= d)
-        def _():
-            g_copy(level).wait_send()
+    def add_in(level):
+        g_copy(level).wait_recv()
+        acc[...] = acc[...] + grecv[level].astype(F32)
+
+    def sent_kv(level):
+        kv_copy(level, 0).wait_send()
+        kv_copy(level, 1).wait_send()
+
+    if with_dw:
+        @pl.when(first)
+        def _():
+            sent_kv(0)
+            add_in(0)
+
+            @pl.when(me >= dist[1])
+            def _():
+                g_copy(0).wait_send()
+
+        @pl.when(second)
+        def _():
+            g_copy(0).wait_send()
+
+            @pl.when(me >= dist[1])
+            def _():
+                sent_kv(0)
+
+        @pl.when((me >= dist[2]) & (me + dist[2] < n))
+        def _():
+            sent_kv(3)
+
+        for level in (1, 2, 3):
+            @pl.when(me + dist[level] < n)
+            def _():
+                if level < 3:
+                    sent_kv(level)
+                add_in(level)
+
+            @pl.when(me >= dist[level])
+            def _():
+                g_copy(level).wait_send()
+    else:
+        for level, d in enumerate(dist):
+            @pl.when(me + d < n)
+            def _():
+                sent_kv(level)
+                add_in(level)
+
+            @pl.when(me >= d)
+            def _():
+                g_copy(level).wait_send()
 
     dk_out[...] = acc[0].astype(BF)
     dv_out[...] = acc[1].astype(BF)

time: 35.5 us -> 32.8 us (0.924)
  Pallas kernels: 34.8 us -> 32 us
    pallas_call x1, Pallas kernels: 33.9 us -> 31.1 us  [shards(): pl.pallas_call(functools.partial(kernel, (n, tp, with_dw)), out_shape=[pl...]
where the time goes in v2:
time: 32.8 us; the launch traced here: 32.6 us
  Pallas kernels  32 us (98%)
  between operations  0.64 us (2%)
    pallas_call x1, Pallas kernels, shards(): pl.pallas_call(functools.partial(kernel, (n, tp, with_dw)), out_shape=[pl...  31.1 us
    pallas_call x1, Pallas kernels, shards(): pl.pallas_call(writer, out_shape=out_shape, in_specs=[vm] * len(out_shape...  0.84 us

profile of v2, /device:TPU:0, one launch (start us, length us, event | category | flops | bytes accessed | tf_op | source)
XLA Modules:
  0.0 32.6 jit_solution(13621957657281262182)
XLA Ops:
  0.6 31.1 %shard_map.111 = (bf16[192,512]{1,0:T(8,128)(2,1)S(1)}, bf16[192,128]{1,0:T(8,128)(2,1)S(1)}, bf16[192,128]{1,0:T(8,128)(2,1)S(1)}, f32[128,512]{1,0:T(8,128)S(1)}) custom-call(bf16[192,128]{1,0:T(8,128)(2,1)} %refs_0_.1, bf16[192,128]{1,0:T(8,128)(2,1)} %refs_1_.1, bf16[192,512]{1,0:T(8,128)(2,1)} %refs_2_.1, bf16[192,1024]{1,0:T(8,128)(2,1)} %refs_3_.1, ...), custom_call_target="tpu_custom_call" | custom-call | tf_op jit(solution)/shard_map/pallas_call | solution.py:528
  31.8 0.8 %shard_map.112 = (bf16[192,512]{1,0:T(8,128)(2,1)}, bf16[192,128]{1,0:T(8,128)(2,1)}, bf16[192,128]{1,0:T(8,128)(2,1)}, f32[128,512]{1,0:T(8,128)}) custom-call(bf16[192,512]{1,0:T(8,128)(2,1)S(1)} %get-tuple-element.8.refs_0_, bf16[192,128]{1,0:T(8,128)(2,1)S(1)} %get-tuple-element.9.refs_1_, bf16[192,128]{1,0:T(8,128)(2,1)S(1)} %get-tuple-element.10.refs_2_, ...), custom_call_target="tpu_custom_call" | custom-call | tf_op jit(solution)/shard_map/pallas_call | solution.py:537

commit v3 on v2

--- a/solution.py
+++ b/solution.py
@@ -174,69 +174,85 @@
     pick = (lax.broadcasted_iota(jnp.int32, (16, qh * DH), 1) // DH
             == lax.broadcasted_iota(jnp.int32, (16, qh * DH), 0)).astype(F32).astype(BF)
     delta_t = dot(pick, hi, NT) + dot(pick, lo, NT)
+    part_cols = grp * BLOCK
     for h in range(kvh):
         for g in range(grp):
             i = h * grp + g
-            lrow[h, 0:1, g * tok:(g + 1) * tok] = lse_t[i:i + 1, 0:tok]
-            drow[h, 0:1, g * tok:(g + 1) * tok] = delta_t[i:i + 1, :]
-            qs[h, g * tok:(g + 1) * tok, :] = q_ref[:, i * DH:(i + 1) * DH]
-            gs[h, g * tok:(g + 1) * tok, :] = g_ref[:, i * DH:(i + 1) * DH]
-
-    q_block = lax.rem(lax.broadcasted_iota(jnp.int32, (1, cols), 1), tok) // BLOCK
-
-    def run_pass(h, k, v, bias):
-        lse = lrow[h, 0:1, :]
-        st = dot(k, qs[h], NT) * (scale * LOG2E)
-        if bias is None:
-            kp = lax.broadcasted_iota(jnp.int32, (tok, cols), 0)
-            qp = lax.rem(lax.broadcasted_iota(jnp.int32, (tok, cols), 1), tok)
-            keep = (qp >= kp) & ((qp // BLOCK) == (kp // BLOCK))
-            p = jnp.exp2(jnp.where(keep, st + lse, NEG))
-        else:
-            p = jnp.concatenate(
-                [jnp.exp2(st[b * BLOCK:(b + 1) * BLOCK] + (lse + bias[b])) for b in range(nb)], axis=0)
-        dp = dot(v, gs[h], NT)
-        ds = (p * (dp - drow[h, 0:1, :])).astype(BF)
-        dv = dot(p.astype(BF), gs[h], NN)
-        dk = dot(ds, qs[h], NN) * scale
-        dq = dot(k, ds, TN)
+            for qb in range(nb):
+                rows_ = slice(qb * BLOCK, (qb + 1) * BLOCK)
+                to = slice(qb * part_cols + g * BLOCK, qb * part_cols + (g + 1) * BLOCK)
+                lrow[h, 0:1, to] = lse_t[i:i + 1, rows_]
+                drow[h, 0:1, to] = delta_t[i:i + 1, rows_]
+                qs[h, to, :] = q_ref[rows_, i * DH:(i + 1) * DH]
+                gs[h, to, :] = g_ref[rows_, i * DH:(i + 1) * DH]
+
+    def run_pass(h, ks, vs, keep):
+        to = [slice(qb * part_cols, (qb + 1) * part_cols) for qb in range(nb)]
+        st = [dot(k, qs[h, t, :], NT) for k, t in zip(ks, to)]
+        dp = [dot(v, gs[h, t, :], NT) for v, t in zip(vs, to)]
+        st = [x * (scale * LOG2E) + lrow[h, 0:1, t] for x, t in zip(st, to)]
+        p = [jnp.exp2(x if keep is None else jnp.where(keep, x, NEG)) for x in st]
+        ds = [(x * (y - drow[h, 0:1, t])).astype(BF) for x, y, t in zip(p, dp, to)]
+        dv = [dot(x.astype(BF), gs[h, t, :], NN) for x, t in zip(p, to)]
+        dq = [dot(k, x, TN) for k, x in zip(ks, ds)]
+        dk = [dot(x, qs[h, t, :], NN) for x, t in zip(ds, to)]
         return dq, dk, dv
 
+    causal = (lax.rem(lax.broadcasted_iota(jnp.int32, (BLOCK, part_cols), 1), BLOCK)
+              >= lax.broadcasted_iota(jnp.int32, (BLOCK, part_cols), 0))
     for h in range(kvh):
         lanes = slice(h * DH, (h + 1) * DH)
-        dq, dk, dv = run_pass(h, k_ref[:, lanes], v_ref[:, lanes], None)
-        dqt[h] = dq
-        acc[0, :, lanes] = dk
-        acc[1, :, lanes] = dv
-
-    def level_bias(level):
-        bias = []
-        for kb in range(nb):
-            row = jnp.full((1, cols), NEG, F32)
-            target = (me - span(level)) * nb + kb
-            for qb in range(nb):
-                hit = jnp.float32(NEG)
-                for i in range(PER):
-                    hit = jnp.where(ch_ref[PER * level + i, me * nb + qb] == target, jnp.float32(0.0), hit)
-                row = jnp.where(q_block == qb, hit, row)
-            bias.append(row)
-        return bias
-
-    def far_pass(level, h, bias):
+        blocks = [slice(qb * BLOCK, (qb + 1) * BLOCK) for qb in range(nb)]
+        dq, dk, dv = run_pass(h, [k_ref[r, lanes] for r in blocks], [v_ref[r, lanes] for r in blocks], causal)
+        dqt[h] = jnp.concatenate(dq, axis=1)
+        acc[0, :, lanes] = jnp.concatenate(dk, axis=0) * scale
+        acc[1, :, lanes] = jnp.concatenate(dv, axis=0)
+
+    def picks(level):
+        found = []
+        for qb in range(nb):
+            pair_ = [jnp.clip(ch_ref[PER * level + i, me * nb + qb] - (me - span(level)) * nb, 0, nb - 1)
+                     for i in range(PER)]
+            found.append((jnp.minimum(*pair_), jnp.maximum(*pair_)))
+        return found
+
+    def far_pass(level, h, found):
         lanes = slice(h * DH, (h + 1) * DH)
-        dq, dk, dv = run_pass(h, kvbuf[level, 0, :, lanes], kvbuf[level, 1, :, lanes], bias)
-        dqt[h] = dqt[h] + dq
-        gsend[level, 0, :, lanes] = dk.astype(BF)
-        gsend[level, 1, :, lanes] = dv.astype(BF)
+        ks, vs = [], []
+        for i, picked in enumerate((ks, vs)):
+            blocks = [kvbuf[level, i, b * BLOCK:(b + 1) * BLOCK, lanes] for b in range(nb)]
+            for low, high in found:
+                first_, second_ = blocks[0], blocks[1]
+                for b in range(1, nb - 1):
+                    first_ = jnp.where(low == b, blocks[b], first_)
+                for b in range(2, nb):
+                    second_ = jnp.where(high == b, blocks[b], second_)
+                picked.append(jnp.concatenate([first_, second_], axis=0))
+        dq, dk, dv = run_pass(h, ks, vs, None)
+        dqt[h] = dqt[h] + jnp.concatenate(dq, axis=1)
+        for i, new in enumerate((dk, dv)):
+            for b in range(nb):
+                total = None
+                for qb in range(nb):
+                    low, high = found[qb]
+                    add = jnp.zeros((BLOCK, DH), F32)
+                    if b:
+                        add = jnp.where(high == b, new[qb][BLOCK:], add)
+                    if b < nb - 1:
+                        add = jnp.where(low == b, new[qb][:BLOCK], add)
+                    total = add if total is None else total + add
+                if i == 0:
+                    total = total * scale
+                gsend[level, i, b * BLOCK:(b + 1) * BLOCK, lanes] = total.astype(BF)
 
     def wait_kv(level):
         kv_copy(level, 0).wait_recv()
         kv_copy(level, 1).wait_recv()
 
     def far_level(level):
-        bias = level_bias(level)
+        found = picks(level)
         for h in range(kvh):
-            far_pass(level, h, bias)
+            far_pass(level, h, found)
 
     def arrive(level):
         wait_kv(level)
@@ -305,14 +321,19 @@
         def _():
             if h == 0:
                 arrive(last)
-            far_pass(last, h, level_bias(last))
-        whole = dqt[h] * scale
-        for g in range(grp):
-            low = whole[:, g * tok:(g + 1) * tok].T.astype(BF)
-            i = h * grp + g
-            dq_out[:, i * DH:(i + 1) * DH] = low
-            if with_dw:
-                dqall[h, mine, g * DH:(g + 1) * DH] = low
+            far_pass(last, h, picks(last))
+        whole = (dqt[h] * scale).astype(BF)
+        step = 2 if grp % 2 == 0 else 1
+        for qb in range(nb):
+            for g in range(0, grp, step):
+                at = qb * part_cols + g * BLOCK
+                low = jnp.concatenate(
+                    [whole[:, at + j * BLOCK:at + (j + 1) * BLOCK] for j in range(step)], axis=0).T
+                i = h * grp + g
+                dq_out[qb * BLOCK:(qb + 1) * BLOCK, i * DH:(i + step) * DH] = low
+                if with_dw:
+                    at_rows = pl.ds(pl.multiple_of(w * tok + qb * BLOCK, BLOCK), BLOCK)
+                    dqall[h, at_rows, g * DH:(g + step) * DH] = low
         if with_dw:
             for s in hops:
                 a_copy(h, s).start()
@@ -352,6 +373,10 @@
                 src_ref=part.at[h, i], dst_ref=precv.at[h, i],
                 send_sem=w_s.at[h, i], recv_sem=w_r.at[h, i],
                 device_id={"kv": (far if i == 2 else near) * wn + w}, device_id_type=pl.DeviceIdType.MESH)
+
+        def send_near(h):
+            part[h, 1] = dot(xt[near], dqall[h], NN).astype(BF)
+            w_copy(h, 1).start()
 
         for h in range(kvh):
             for s in hops:
@@ -366,8 +391,6 @@
                 f_copy(h, s).wait_recv()
             part[h, 0] = dot(xt[lax.rem(near + 2, zn)], dqall[h], NN).astype(BF)
             w_copy(h, 0).start()
-            part[h, 1] = dot(xt[near], dqall[h], NN).astype(BF)
-            w_copy(h, 1).start()
         @pl.when(w >= 2)
         def _():
             early_sum()
@@ -375,11 +398,14 @@
         x_arrive(1)
         for zz in (far, z):
             xt[zz] = xbuf[zz].T
+        send_near(0)
         for h in range(kvh):
             ours = dot(xt[far], dqall[h], NN)
             w_copy(h, 0).wait_recv()
             part[h, 2] = (ours + precv[h, 0].astype(F32)).astype(BF)
             w_copy(h, 2).start()
+            if h + 1 < kvh:
+                send_near(h + 1)
         width = grp * DH
         for h in range(kvh):
             dw_out[:, h * width:(h + 1) * width] = dot(xt[z], dqall[h], NN)

time: 32.8 us -> 31.6 us (0.963)
  Pallas kernels: 32 us -> 30.8 us
    pallas_call x1, Pallas kernels: 31.1 us -> 29.9 us  [shards(): pl.pallas_call(functools.partial(kernel, (n, tp, with_dw)), out_shape=[pl...]
where the time goes in v3:
time: 31.6 us; the launch traced here: 31.4 us
  Pallas kernels  30.8 us (97%)
  between operations  0.64 us (2%)
    pallas_call x1, Pallas kernels, shards(): pl.pallas_call(functools.partial(kernel, (n, tp, with_dw)), out_shape=[pl...  29.9 us
    pallas_call x1, Pallas kernels, shards(): pl.pallas_call(writer, out_shape=out_shape, in_specs=[vm] * len(out_shape...  0.84 us

profile of v3, /device:TPU:0, one launch (start us, length us, event | category | flops | bytes accessed | tf_op | source)
XLA Modules:
  0.0 31.4 jit_solution(10025207677686939662)
XLA Ops:
  0.6 29.9 %shard_map.111 = (bf16[192,512]{1,0:T(8,128)(2,1)S(1)}, bf16[192,128]{1,0:T(8,128)(2,1)S(1)}, bf16[192,128]{1,0:T(8,128)(2,1)S(1)}, f32[128,512]{1,0:T(8,128)S(1)}) custom-call(bf16[192,128]{1,0:T(8,128)(2,1)} %refs_0_.1, bf16[192,128]{1,0:T(8,128)(2,1)} %refs_1_.1, bf16[192,512]{1,0:T(8,128)(2,1)} %refs_2_.1, bf16[192,1024]{1,0:T(8,128)(2,1)} %refs_3_.1, ...), custom_call_target="tpu_custom_call" | custom-call | tf_op jit(solution)/shard_map/pallas_call | solution.py:554
  30.6 0.8 %shard_map.112 = (bf16[192,512]{1,0:T(8,128)(2,1)}, bf16[192,128]{1,0:T(8,128)(2,1)}, bf16[192,128]{1,0:T(8,128)(2,1)}, f32[128,512]{1,0:T(8,128)}) custom-call(bf16[192,512]{1,0:T(8,128)(2,1)S(1)} %get-tuple-element.8.refs_0_, bf16[192,128]{1,0:T(8,128)(2,1)S(1)} %get-tuple-element.9.refs_1_, bf16[192,128]{1,0:T(8,128)(2,1)S(1)} %get-tuple-element.10.refs_2_, ...), custom_call_target="tpu_custom_call" | custom-call | tf_op jit(solution)/shard_map/pallas_call | solution.py:563

commit v4 on v3

--- a/solution.py
+++ b/solution.py
@@ -32,20 +32,26 @@
     ch_hbm, refs = refs[0], refs[1:]
     count_out = 4 if with_dw else 3
     outs, refs = refs[:count_out], refs[count_out:]
-    held, refs = refs[:count_in], refs[count_in:]
+    kv_ref, qgo, lse_ref, refs = refs[0], refs[1], refs[2], refs[3:]
+    if with_dw:
+        x_ref, refs = refs[0], refs[1:]
     ch_ref, refs = refs[0], refs[1:]
     (in_s, qs, gs, lrow, drow, dqt, acc, kvbuf, gsend, grecv,
      kv_s, kv_r, g_s, g_r) = refs[:14]
     dq_out, dk_out, dv_out = outs[:3]
-    k_ref, v_ref, q_ref, g_ref, o_ref, lse_ref = held[:3] + held[-3:]
-    if with_dw:
-        x_ref = held[3]
+    k_ref, v_ref = kv_ref.at[0], kv_ref.at[1]
+    q_ref, g_ref, o_ref = qgo.at[0], qgo.at[1], qgo.at[2]
+    if with_dw:
         dw_out = outs[3]
-        (xbuf, xt, dqall, part, precv, x_s, x_r, a_s, a_r, f_s, f_r, w_s, w_r) = refs[14:]
-    loads = [pltpu.make_async_copy(hbm[i], held[i], in_s.at[i]) for i in range(count_in)]
-    loads.append(pltpu.make_async_copy(ch_hbm, ch_ref, in_s.at[count_in]))
-    for load in loads:
-        load.start()
+        (xbuf, xt, dqall, part, precv, x_s, x_r, a_s, a_r, w_s, w_r) = refs[14:]
+    places = [k_ref, v_ref, q_ref, g_ref, o_ref, lse_ref] + ([x_ref] if with_dw else [])
+    for i, to in enumerate(places):
+        pltpu.make_async_copy(hbm[i], to, in_s.at[(0, 0, 1, 1, 1, 2, 4)[i]]).start()
+    pltpu.make_async_copy(ch_hbm, ch_ref, in_s.at[3]).start()
+
+    def drain(ref, sem):
+        pltpu.make_async_copy(ref, ref, sem).wait()
+
     me = lax.axis_index("kv")
     mt = lax.axis_index("tp")
     tok = q_ref.shape[0]
@@ -74,6 +80,10 @@
         across_pair = lax.rem(pair + 2, wn)
         near = z + 1 - 2 * lax.rem(z, 2)
         far = lax.rem(z + 2, zn)
+        outer = (z == 0) | (z == zn - 1)
+        inner = (z > 0) & (z < zn - 1)
+        to_outer = jnp.where(outer, zn - 1 - z, zn - 1 - near)
+        to_inner = jnp.where(outer, zn - 1 - near, zn - 1 - z)
         partner = me + 1 - 2 * lax.rem(me, 2)
         first = lax.rem(me, 2) == 0
         second = lax.rem(me, 2) == 1
@@ -100,17 +110,16 @@
         count = count + len(plane) + 2
     pl.semaphore_wait(barrier, count)
 
-    def kv_copy(level, i):
+    def kv_copy(level):
         return pltpu.make_async_remote_copy(
-            src_ref=(k_ref, v_ref)[i], dst_ref=kvbuf.at[level, i],
-            send_sem=kv_s.at[level, i], recv_sem=kv_r.at[level, i],
+            src_ref=kv_ref, dst_ref=kvbuf.at[level],
+            send_sem=kv_s.at[level], recv_sem=kv_r.at[level],
             device_id={"kv": me + span(level)}, device_id_type=pl.DeviceIdType.MESH)
 
-    def kv_pass_on(level, i, held_kv):
-        to, src = (0, held_kv) if level == 0 else (3, kvbuf.at[2, i])
+    def kv_pass_on(level, src):
         return pltpu.make_async_remote_copy(
-            src_ref=src, dst_ref=kvbuf.at[to, i],
-            send_sem=kv_s.at[to, i], recv_sem=kv_r.at[to, i],
+            src_ref=src, dst_ref=kvbuf.at[level],
+            send_sem=kv_s.at[level], recv_sem=kv_r.at[level],
             device_id={"kv": partner if level == 0 else me + dist[2]}, device_id_type=pl.DeviceIdType.MESH)
 
     def g_copy(level):
@@ -120,8 +129,7 @@
             send_sem=g_s.at[level], recv_sem=g_r.at[level],
             device_id={"kv": to}, device_id_type=pl.DeviceIdType.MESH)
 
-    loads[0].wait()
-    loads[1].wait()
+    drain(kv_ref, in_s.at[0])
     turns = [0, 1, 3, 2]
     if with_dw:
         late = w == 0
@@ -130,14 +138,12 @@
     for level in (2, 1) if with_dw else turns:
         @pl.when(me + dist[level] < n)
         def _():
-            kv_copy(level, 0).start()
-            kv_copy(level, 1).start()
+            kv_copy(level).start()
 
     if with_dw:
         @pl.when(first)
         def _():
-            kv_pass_on(0, 0, k_ref).start()
-            kv_pass_on(0, 1, v_ref).start()
+            kv_pass_on(0, kv_ref).start()
 
         def x_copy(idx, k):
             wt, tt = plane[idx]
@@ -146,27 +152,27 @@
             return pltpu.make_async_remote_copy(
                 src_ref=x_ref.at[:, pl.ds(off, rows)],
                 dst_ref=xbuf.at[mt * zper + zz, pl.ds(pl.multiple_of(w * tok, tok), tok)],
-                send_sem=x_s.at[idx, k], recv_sem=x_r.at[idx, k],
+                send_sem=x_s.at[0 if idx else 1], recv_sem=x_r.at[k, 0 if idx in (1, 2) else 1],
                 device_id={"kv": z * wn + wt, "tp": tt}, device_id_type=pl.DeviceIdType.MESH)
 
         def x_forward(idx, k):
             slot = xbuf.at[mt * zper + order[k], pl.ds(pl.multiple_of(plane[idx][0] * tok, tok), tok)]
             return pltpu.make_async_remote_copy(
                 src_ref=slot, dst_ref=slot,
-                send_sem=x_s.at[idx + 4, k], recv_sem=x_r.at[idx + 4, k],
+                send_sem=x_s.at[1], recv_sem=x_r.at[k, 2],
                 device_id={"kv": me, "tp": 1 - mt}, device_id_type=pl.DeviceIdType.MESH)
 
-        loads[3].wait()
+        drain(x_ref, in_s.at[4])
         for k in range(zper):
-            for idx in (1, 2, 3, 4, 0):
+            for idx in (3, 4, 0) if k else (1, 2, 3, 4, 0):
                 x_copy(idx, k).start()
         for zz in range(zper):
             off = pl.multiple_of((zz * wn + w) * rows, rows)
             xbuf[mt * zper + zz, pl.ds(pl.multiple_of(w * tok, tok), tok), :] = x_ref[:, pl.ds(off, rows)]
 
-    for i in range(count_in + 1):
-        if i not in (0, 1, 3) or (i == 3 and not with_dw):
-            loads[i].wait()
+    drain(qgo, in_s.at[1])
+    drain(lse_ref, in_s.at[2])
+    pltpu.make_async_copy(ch_hbm, ch_ref, in_s.at[3]).wait()
     lse_t = lse_ref[...] * (-LOG2E)
     prod = g_ref[...].astype(F32) * o_ref[...].astype(F32)
     hi = prod.astype(BF)
@@ -246,8 +252,7 @@
                 gsend[level, i, b * BLOCK:(b + 1) * BLOCK, lanes] = total.astype(BF)
 
     def wait_kv(level):
-        kv_copy(level, 0).wait_recv()
-        kv_copy(level, 1).wait_recv()
+        kv_copy(level).wait_recv()
 
     def far_level(level):
         found = picks(level)
@@ -259,13 +264,11 @@
         if with_dw:
             @pl.when((level == 2) & (me + dist[2] < n))
             def _():
-                kv_pass_on(3, 0, None).start()
-                kv_pass_on(3, 1, None).start()
+                kv_pass_on(3, kvbuf.at[2]).start()
 
             @pl.when((level == 1) & second)
             def _():
-                kv_pass_on(0, 0, kvbuf.at[1, 0]).start()
-                kv_pass_on(0, 1, kvbuf.at[1, 1]).start()
+                kv_pass_on(0, kvbuf.at[1]).start()
 
     def return_level(level):
         if with_dw:
@@ -276,11 +279,15 @@
             g_copy(level).start()
 
     def pass_x_on(k):
+        drain(xbuf.at[0, 0:2 * tok], x_r.at[k, 0])
         for idx in (1, 2):
-            x_copy(idx, k).wait_recv()
             x_forward(idx, k).start()
 
     for turn, level in enumerate(turns[:-1]):
+        if with_dw and turn == 1:
+            x_copy(1, 1).start()
+            x_copy(2, 1).start()
+
         if with_dw and turn == 2:
             @pl.when((z >= 1) & first)
             def _():
@@ -300,14 +307,14 @@
             to = pair if s == 0 else lax.rem(w + s, wn)
             return pltpu.make_async_remote_copy(
                 src_ref=dqall.at[h, mine], dst_ref=dqall.at[h, mine],
-                send_sem=a_s.at[h, s // 2], recv_sem=a_r.at[h, s // 2],
+                send_sem=a_s, recv_sem=a_r.at[h, s // 2],
                 device_id={"kv": z * wn + to}, device_id_type=pl.DeviceIdType.MESH)
 
         def f_copy(h, s):
             slot = pl.ds(pl.multiple_of(lax.rem(w + wn - s, wn) * tok, tok), tok)
             return pltpu.make_async_remote_copy(
                 src_ref=dqall.at[h, slot], dst_ref=dqall.at[h, slot],
-                send_sem=f_s.at[h, s // 2 - 1], recv_sem=f_r.at[h, s // 2 - 1],
+                send_sem=a_s, recv_sem=a_r.at[h, 0],
                 device_id={"kv": z * wn + pair}, device_id_type=pl.DeviceIdType.MESH)
 
     if with_dw:
@@ -363,70 +370,91 @@
             early_sum()
 
         def x_arrive(k):
-            for idx in (0, 3, 4):
-                x_copy(idx, k).wait_recv()
-            for idx in (1, 2):
-                x_forward(idx, k).wait_recv()
-
-        def w_copy(h, i):
+            drain(xbuf.at[0, 0:3 * tok], x_r.at[k, 1])
+            drain(xbuf.at[0, 0:2 * tok], x_r.at[k, 2])
+
+        def w_copy(h, i, slot, to):
             return pltpu.make_async_remote_copy(
-                src_ref=part.at[h, i], dst_ref=precv.at[h, i],
-                send_sem=w_s.at[h, i], recv_sem=w_r.at[h, i],
-                device_id={"kv": (far if i == 2 else near) * wn + w}, device_id_type=pl.DeviceIdType.MESH)
-
-        def send_near(h):
-            part[h, 1] = dot(xt[near], dqall[h], NN).astype(BF)
-            w_copy(h, 1).start()
-
-        for h in range(kvh):
+                src_ref=part.at[h, i], dst_ref=precv.at[h, slot],
+                send_sem=w_s, recv_sem=w_r.at[h, slot],
+                device_id={"kv": to * wn + w}, device_id_type=pl.DeviceIdType.MESH)
+
+        def w_arrive(h, slot):
+            w_copy(h, 1, slot, near).wait_recv()
+
+        def send_part(h, i, slot, block, to, add=None):
+            new = dot(xt[block], dqall[h], NN)
+            if add is not None:
+                w_arrive(h, add)
+                new = new + precv[h, add].astype(F32)
+            part[h, i] = new.astype(BF)
+            w_copy(h, i, slot, to).start()
+
+        def across_on(h):
             for s in hops:
                 a_copy(h, s).wait_recv()
                 f_copy(h, s).start()
+
+        for h in range(kvh):
             if h == 0:
-                x_arrive(0)
-                for zz in (lax.rem(near + 2, zn), near):
+                across_on(h)
+
+                @pl.when(second)
+                def _():
+                    for later in range(1, kvh):
+                        across_on(later)
+            else:
+                @pl.when(first)
+                def _():
+                    across_on(h)
+            if h < zper:
+                x_arrive(h)
+                for zz in ((lax.rem(near + 2, zn), near), (far, z))[h]:
                     xt[zz] = xbuf[zz].T
-            a_copy(h, 0).wait_recv()
-            for s in hops:
-                f_copy(h, s).wait_recv()
-            part[h, 0] = dot(xt[lax.rem(near + 2, zn)], dqall[h], NN).astype(BF)
-            w_copy(h, 0).start()
+            if h == 1:
+                @pl.when(outer)
+                def _():
+                    send_part(0, 2, 3, to_inner, near)
+
+            drain(dqall.at[h, 0:2 * tok], a_r.at[h, 0])
+            @pl.when(outer)
+            def _():
+                send_part(h, 0, 0, to_outer, near)
+                if h:
+                    send_part(h, 2, 3, to_inner, near)
+
+            @pl.when(inner)
+            def _():
+                send_part(h, 1, 1, near, near)
+
         @pl.when(w >= 2)
         def _():
             early_sum()
 
-        x_arrive(1)
-        for zz in (far, z):
-            xt[zz] = xbuf[zz].T
-        send_near(0)
+        @pl.when(outer)
+        def _():
+            for h in range(kvh):
+                send_part(h, 1, 1, near, near)
+
         for h in range(kvh):
-            ours = dot(xt[far], dqall[h], NN)
-            w_copy(h, 0).wait_recv()
-            part[h, 2] = (ours + precv[h, 0].astype(F32)).astype(BF)
-            w_copy(h, 2).start()
-            if h + 1 < kvh:
-                send_near(h + 1)
+            @pl.when(inner)
+            def _():
+                send_part(h, 0, 2, to_outer, to_outer, 0)
+                send_part(h, 2, 2, to_inner, to_inner, 3)
+
         width = grp * DH
         for h in range(kvh):
             dw_out[:, h * width:(h + 1) * width] = dot(xt[z], dqall[h], NN)
-        for k in range(zper):
-            for idx in range(len(plane)):
-                x_copy(idx, k).wait_send()
-            for idx in (1, 2):
-                x_forward(idx, k).wait_send()
-        for h in range(kvh):
-            for s in [0] + hops:
-                a_copy(h, s).wait_send()
-            for s in hops:
-                f_copy(h, s).wait_send()
+        drain(xbuf.at[0:2], x_s.at[0])
+        drain(xbuf.at[0:3, 0:2 * tok], x_s.at[1])
+        drain(dqall.at[:, 0:3 * tok], a_s)
 
     def add_in(level):
         g_copy(level).wait_recv()
         acc[...] = acc[...] + grecv[level].astype(F32)
 
     def sent_kv(level):
-        kv_copy(level, 0).wait_send()
-        kv_copy(level, 1).wait_send()
+        kv_copy(level).wait_send()
 
     if with_dw:
         @pl.when(first)
@@ -476,10 +504,10 @@
     if with_dw:
         for h in range(kvh):
             lanes = slice(h * width, (h + 1) * width)
-            w_copy(h, 0).wait_send()
-            w_copy(h, 1).wait()
-            w_copy(h, 2).wait()
+            w_arrive(h, 1)
+            w_arrive(h, 2)
             dw_out[:, lanes] = dw_out[:, lanes] + precv[h, 1].astype(F32) + precv[h, 2].astype(F32)
+        drain(part, w_s)
 
 
 def writer(*refs):
@@ -512,10 +540,11 @@
     ]
     args = [keys, values, queries, grad_out, attn_out, log_sum.T]
     if with_dw:
-        args.insert(3, layer_input)
-    scratch = [pltpu.VMEM(a.shape, a.dtype) for a in args] + [
+        args.append(layer_input)
+    held = [((2, tok, kw), BF), ((3, tok, qw), BF)] + [(a.shape, a.dtype) for a in args[5:]]
+    scratch = [pltpu.VMEM(*a) for a in held] + [
         pltpu.SMEM(chosen.T.shape, chosen.dtype),
-        pltpu.SemaphoreType.DMA((len(args) + 1,)),
+        pltpu.SemaphoreType.DMA((5,)),
         pltpu.VMEM((kvh, cols, DH), BF),
         pltpu.VMEM((kvh, cols, DH), BF),
         pltpu.VMEM((kvh, 1, cols), F32),
@@ -525,8 +554,8 @@
         pltpu.VMEM((LEVELS, 2, tok, kw), BF),
         pltpu.VMEM((LEVELS, 2, tok, kw), BF),
         pltpu.VMEM((LEVELS, 2, tok, kw), BF),
-        pltpu.SemaphoreType.DMA((LEVELS, 2)),
-        pltpu.SemaphoreType.DMA((LEVELS, 2)),
+        pltpu.SemaphoreType.DMA((LEVELS,)),
+        pltpu.SemaphoreType.DMA((LEVELS,)),
         pltpu.SemaphoreType.DMA((LEVELS,)),
         pltpu.SemaphoreType.DMA((LEVELS,)),
     ]
@@ -534,22 +563,19 @@
     specs = [hbm] * (len(args) + 1)
     if with_dw:
         out_shape.append(jax.ShapeDtypeStruct((rows, qw), F32))
-        peers = 7
         zper = zn // tp
         scratch += [
             pltpu.VMEM((zn, wn * tok, rows), BF),
             pltpu.VMEM((zn, rows, wn * tok), BF),
             pltpu.VMEM((kvh, wn * tok, qw // kvh), BF),
             pltpu.VMEM((kvh, zn - 1, rows, qw // kvh), BF),
-            pltpu.VMEM((kvh, zn - 1, rows, qw // kvh), BF),
-            pltpu.SemaphoreType.DMA((peers, zper)),
-            pltpu.SemaphoreType.DMA((peers, zper)),
-            pltpu.SemaphoreType.DMA((kvh, wn // 2)),
-            pltpu.SemaphoreType.DMA((kvh, wn // 2)),
-            pltpu.SemaphoreType.DMA((kvh, max(wn // 2 - 1, 1))),
-            pltpu.SemaphoreType.DMA((kvh, max(wn // 2 - 1, 1))),
-            pltpu.SemaphoreType.DMA((kvh, zn - 1)),
-            pltpu.SemaphoreType.DMA((kvh, zn - 1)),
+            pltpu.VMEM((kvh, zn, rows, qw // kvh), BF),
+            pltpu.SemaphoreType.DMA((2,)),
+            pltpu.SemaphoreType.DMA((zper, 3)),
+            pltpu.SemaphoreType.DMA,
+            pltpu.SemaphoreType.DMA((kvh, 2)),
+            pltpu.SemaphoreType.DMA,
+            pltpu.SemaphoreType.DMA((kvh, zn)),
         ]
     outs = pl.pallas_call(
         functools.partial(kernel, (n, tp, with_dw)),

time: 31.6 us -> 31.1 us (0.984)
  Pallas kernels: 30.8 us -> 30.3 us
    pallas_call x1, Pallas kernels: 29.9 us -> 29.5 us  [shards(): pl.pallas_call(functools.partial(kernel, (n, tp, with_dw)), out_shape=[pl...]
where the time goes in v4:
time: 31.1 us; the launch traced here: 30.9 us
  Pallas kernels  30.3 us (97%)
  between operations  0.64 us (2%)
    pallas_call x1, Pallas kernels, shards(): pl.pallas_call(functools.partial(kernel, (n, tp, with_dw)), out_shape=[pl...  29.5 us
    pallas_call x1, Pallas kernels, shards(): pl.pallas_call(writer, out_shape=out_shape, in_specs=[vm] * len(out_shape...  0.84 us

profile of v4, /device:TPU:0, one launch (start us, length us, event | category | flops | bytes accessed | tf_op | source)
XLA Modules:
  0.0 30.9 jit_solution(15682276964539857613)
XLA Ops:
  0.6 29.5 %shard_map.111 = (bf16[192,512]{1,0:T(8,128)(2,1)S(1)}, bf16[192,128]{1,0:T(8,128)(2,1)S(1)}, bf16[192,128]{1,0:T(8,128)(2,1)S(1)}, f32[128,512]{1,0:T(8,128)S(1)}) custom-call(bf16[192,128]{1,0:T(8,128)(2,1)} %refs_0_.1, bf16[192,128]{1,0:T(8,128)(2,1)} %refs_1_.1, bf16[192,512]{1,0:T(8,128)(2,1)} %refs_2_.1, bf16[192,512]{1,0:T(8,128)(2,1)} %refs_3_.1, ...), custom_call_target="tpu_custom_call" | custom-call | tf_op jit(solution)/shard_map/pallas_call | solution.py:580
  30.1 0.8 %shard_map.112 = (bf16[192,512]{1,0:T(8,128)(2,1)}, bf16[192,128]{1,0:T(8,128)(2,1)}, bf16[192,128]{1,0:T(8,128)(2,1)}, f32[128,512]{1,0:T(8,128)}) custom-call(bf16[192,512]{1,0:T(8,128)(2,1)S(1)} %get-tuple-element.8.refs_0_, bf16[192,128]{1,0:T(8,128)(2,1)S(1)} %get-tuple-element.9.refs_1_, bf16[192,128]{1,0:T(8,128)(2,1)S(1)} %get-tuple-element.10.refs_2_, ...), custom_call_target="tpu_custom_call" | custom-call | tf_op jit(solution)/shard_map/pallas_call | solution.py:589

commit v5 on v4

--- a/solution.py
+++ b/solution.py
@@ -192,27 +192,29 @@
                 qs[h, to, :] = q_ref[rows_, i * DH:(i + 1) * DH]
                 gs[h, to, :] = g_ref[rows_, i * DH:(i + 1) * DH]
 
-    def run_pass(h, ks, vs, keep):
+    def run_pass(heads, ks, vs, keep):
         to = [slice(qb * part_cols, (qb + 1) * part_cols) for qb in range(nb)]
-        st = [dot(k, qs[h, t, :], NT) for k, t in zip(ks, to)]
-        dp = [dot(v, gs[h, t, :], NT) for v, t in zip(vs, to)]
-        st = [x * (scale * LOG2E) + lrow[h, 0:1, t] for x, t in zip(st, to)]
+        each = [(h, t, k, v) for h, hk, hv in zip(heads, ks, vs) for t, k, v in zip(to, hk, hv)]
+        st = [dot(k, qs[h, t, :], NT) for h, t, k, v in each]
+        dp = [dot(v, gs[h, t, :], NT) for h, t, k, v in each]
+        st = [x * (scale * LOG2E) + lrow[h, 0:1, t] for x, (h, t, k, v) in zip(st, each)]
         p = [jnp.exp2(x if keep is None else jnp.where(keep, x, NEG)) for x in st]
-        ds = [(x * (y - drow[h, 0:1, t])).astype(BF) for x, y, t in zip(p, dp, to)]
-        dv = [dot(x.astype(BF), gs[h, t, :], NN) for x, t in zip(p, to)]
-        dq = [dot(k, x, TN) for k, x in zip(ks, ds)]
-        dk = [dot(x, qs[h, t, :], NN) for x, t in zip(ds, to)]
-        return dq, dk, dv
+        ds = [(x * (y - drow[h, 0:1, t])).astype(BF) for x, y, (h, t, k, v) in zip(p, dp, each)]
+        dv = [dot(x.astype(BF), gs[h, t, :], NN) for x, (h, t, k, v) in zip(p, each)]
+        dq = [dot(k, x, TN) for x, (h, t, k, v) in zip(ds, each)]
+        dk = [dot(x, qs[h, t, :], NN) for x, (h, t, k, v) in zip(ds, each)]
+        return [(dq[i * nb:(i + 1) * nb], dk[i * nb:(i + 1) * nb], dv[i * nb:(i + 1) * nb]) for i in range(len(heads))]
 
     causal = (lax.rem(lax.broadcasted_iota(jnp.int32, (BLOCK, part_cols), 1), BLOCK)
               >= lax.broadcasted_iota(jnp.int32, (BLOCK, part_cols), 0))
-    for h in range(kvh):
-        lanes = slice(h * DH, (h + 1) * DH)
-        blocks = [slice(qb * BLOCK, (qb + 1) * BLOCK) for qb in range(nb)]
-        dq, dk, dv = run_pass(h, [k_ref[r, lanes] for r in blocks], [v_ref[r, lanes] for r in blocks], causal)
+    blocks = [slice(qb * BLOCK, (qb + 1) * BLOCK) for qb in range(nb)]
+    lanes_of = [slice(h * DH, (h + 1) * DH) for h in range(kvh)]
+    own = run_pass(list(range(kvh)), [[k_ref[r, l] for r in blocks] for l in lanes_of],
+                   [[v_ref[r, l] for r in blocks] for l in lanes_of], causal)
+    for h, (dq, dk, dv) in enumerate(own):
         dqt[h] = jnp.concatenate(dq, axis=1)
-        acc[0, :, lanes] = jnp.concatenate(dk, axis=0) * scale
-        acc[1, :, lanes] = jnp.concatenate(dv, axis=0)
+        acc[0, :, lanes_of[h]] = jnp.concatenate(dk, axis=0) * scale
+        acc[1, :, lanes_of[h]] = jnp.concatenate(dv, axis=0)
 
     def picks(level):
         found = []
@@ -222,42 +224,43 @@
             found.append((jnp.minimum(*pair_), jnp.maximum(*pair_)))
         return found
 
-    def far_pass(level, h, found):
-        lanes = slice(h * DH, (h + 1) * DH)
+    def far_pass(level, heads, found):
         ks, vs = [], []
         for i, picked in enumerate((ks, vs)):
-            blocks = [kvbuf[level, i, b * BLOCK:(b + 1) * BLOCK, lanes] for b in range(nb)]
-            for low, high in found:
-                first_, second_ = blocks[0], blocks[1]
-                for b in range(1, nb - 1):
-                    first_ = jnp.where(low == b, blocks[b], first_)
-                for b in range(2, nb):
-                    second_ = jnp.where(high == b, blocks[b], second_)
-                picked.append(jnp.concatenate([first_, second_], axis=0))
-        dq, dk, dv = run_pass(h, ks, vs, None)
-        dqt[h] = dqt[h] + jnp.concatenate(dq, axis=1)
-        for i, new in enumerate((dk, dv)):
-            for b in range(nb):
-                total = None
-                for qb in range(nb):
-                    low, high = found[qb]
-                    add = jnp.zeros((BLOCK, DH), F32)
-                    if b:
-                        add = jnp.where(high == b, new[qb][BLOCK:], add)
-                    if b < nb - 1:
-                        add = jnp.where(low == b, new[qb][:BLOCK], add)
-                    total = add if total is None else total + add
-                if i == 0:
-                    total = total * scale
-                gsend[level, i, b * BLOCK:(b + 1) * BLOCK, lanes] = total.astype(BF)
+            for h in heads:
+                blocks = [kvbuf[level, i, b * BLOCK:(b + 1) * BLOCK, lanes_of[h]] for b in range(nb)]
+                chosen_blocks = []
+                for low, high in found:
+                    first_, second_ = blocks[0], blocks[1]
+                    for b in range(1, nb - 1):
+                        first_ = jnp.where(low == b, blocks[b], first_)
+                    for b in range(2, nb):
+                        second_ = jnp.where(high == b, blocks[b], second_)
+                    chosen_blocks.append(jnp.concatenate([first_, second_], axis=0))
+                picked.append(chosen_blocks)
+        for h, (dq, dk, dv) in zip(heads, run_pass(heads, ks, vs, None)):
+            dqt[h] = dqt[h] + jnp.concatenate(dq, axis=1)
+            for i, new in enumerate((dk, dv)):
+                for b in range(nb):
+                    total = None
+                    for qb in range(nb):
+                        low, high = found[qb]
+                        add = jnp.zeros((BLOCK, DH), F32)
+                        if b:
+                            add = jnp.where(high == b, new[qb][BLOCK:], add)
+                        if b < nb - 1:
+                            add = jnp.where(low == b, new[qb][:BLOCK], add)
+                        total = add if total is None else total + add
+                    if i == 0:
+                        total = total * scale
+                    gsend[level, i, b * BLOCK:(b + 1) * BLOCK, lanes_of[h]] = total.astype(BF)
 
     def wait_kv(level):
         kv_copy(level).wait_recv()
 
     def far_level(level):
         found = picks(level)
-        for h in range(kvh):
-            far_pass(level, h, found)
+        far_pass(level, list(range(kvh)), found)
 
     def arrive(level):
         wait_kv(level)
@@ -328,7 +331,7 @@
         def _():
             if h == 0:
                 arrive(last)
-            far_pass(last, h, picks(last))
+            far_pass(last, [h], picks(last))
         whole = (dqt[h] * scale).astype(BF)
         step = 2 if grp % 2 == 0 else 1
         for qb in range(nb):
@@ -411,17 +414,13 @@
                 x_arrive(h)
                 for zz in ((lax.rem(near + 2, zn), near), (far, z))[h]:
                     xt[zz] = xbuf[zz].T
-            if h == 1:
-                @pl.when(outer)
-                def _():
-                    send_part(0, 2, 3, to_inner, near)
-
             drain(dqall.at[h, 0:2 * tok], a_r.at[h, 0])
             @pl.when(outer)
             def _():
                 send_part(h, 0, 0, to_outer, near)
                 if h:
-                    send_part(h, 2, 3, to_inner, near)
+                    for each in range(kvh):
+                        send_part(each, 2, 3, to_inner, near)
 
             @pl.when(inner)
             def _():
@@ -436,10 +435,11 @@
             for h in range(kvh):
                 send_part(h, 1, 1, near, near)
 
-        for h in range(kvh):
-            @pl.when(inner)
-            def _():
+        @pl.when(inner)
+        def _():
+            for h in range(kvh):
                 send_part(h, 0, 2, to_outer, to_outer, 0)
+            for h in range(kvh):
                 send_part(h, 2, 2, to_inner, to_inner, 3)
 
         width = grp * DH

time: 31.1 us -> 30.4 us (0.977)
  the two profiles are of different devices: /device:TPU:0 before, /device:TPU:9 now
where the time goes in v5:
time: 30.4 us; the launch traced here: 30.3 us
  Pallas kernels  29.6 us (97%)
  between operations  0.64 us (2%)
    pallas_call x1, Pallas kernels, shards(): pl.pallas_call(functools.partial(kernel, (n, tp, with_dw)), out_shape=[pl...  28.8 us
    pallas_call x1, Pallas kernels, shards(): pl.pallas_call(writer, out_shape=out_shape, in_specs=[vm] * len(out_shape...  0.84 us

profile of v5, /device:TPU:9, one launch (start us, length us, event | category | flops | bytes accessed | tf_op | source)
XLA Modules:
  0.0 30.3 jit_solution(2009794589992606730)
XLA Ops:
  0.6 28.8 %shard_map.111 = (bf16[192,512]{1,0:T(8,128)(2,1)S(1)}, bf16[192,128]{1,0:T(8,128)(2,1)S(1)}, bf16[192,128]{1,0:T(8,128)(2,1)S(1)}, f32[128,512]{1,0:T(8,128)S(1)}) custom-call(bf16[192,128]{1,0:T(8,128)(2,1)} %refs_0_.1, bf16[192,128]{1,0:T(8,128)(2,1)} %refs_1_.1, bf16[192,512]{1,0:T(8,128)(2,1)} %refs_2_.1, bf16[192,512]{1,0:T(8,128)(2,1)} %refs_3_.1, ...), custom_call_target="tpu_custom_call" | custom-call | tf_op jit(solution)/shard_map/pallas_call | solution.py:580
  29.4 0.8 %shard_map.112 = (bf16[192,512]{1,0:T(8,128)(2,1)}, bf16[192,128]{1,0:T(8,128)(2,1)}, bf16[192,128]{1,0:T(8,128)(2,1)}, f32[128,512]{1,0:T(8,128)}) custom-call(bf16[192,512]{1,0:T(8,128)(2,1)S(1)} %get-tuple-element.8.refs_0_, bf16[192,128]{1,0:T(8,128)(2,1)S(1)} %get-tuple-element.9.refs_1_, bf16[192,128]{1,0:T(8,128)(2,1)S(1)} %get-tuple-element.10.refs_2_, ...), custom_call_target="tpu_custom_call" | custom-call | tf_op jit(solution)/shard_map/pallas_call | solution.py:589

commit v6 on v5

--- a/solution.py
+++ b/solution.py
@@ -136,7 +136,7 @@
         turns = [jnp.where(second, 0, 2), jnp.where(second, 2, jnp.where(late, 0, 1)),
                  jnp.where(second, 1, jnp.where(late, 3, 0)), jnp.where(late, 1, 3)]
     for level in (2, 1) if with_dw else turns:
-        @pl.when(me + dist[level] < n)
+        @pl.when((me + dist[level] < n) & (w < 3) if with_dw and level == 1 else me + dist[level] < n)
         def _():
             kv_copy(level).start()
 
@@ -164,7 +164,7 @@
 
         drain(x_ref, in_s.at[4])
         for k in range(zper):
-            for idx in (3, 4, 0) if k else (1, 2, 3, 4, 0):
+            for idx in (1, 2, 3, 4, 0):
                 x_copy(idx, k).start()
         for zz in range(zper):
             off = pl.multiple_of((zz * wn + w) * rows, rows)
@@ -215,6 +215,11 @@
         dqt[h] = jnp.concatenate(dq, axis=1)
         acc[0, :, lanes_of[h]] = jnp.concatenate(dk, axis=0) * scale
         acc[1, :, lanes_of[h]] = jnp.concatenate(dv, axis=0)
+
+    if with_dw:
+        @pl.when((me + dist[1] < n) & (w == 3))
+        def _():
+            kv_copy(1).start()
 
     def picks(level):
         found = []
@@ -287,10 +292,6 @@
             x_forward(idx, k).start()
 
     for turn, level in enumerate(turns[:-1]):
-        if with_dw and turn == 1:
-            x_copy(1, 1).start()
-            x_copy(2, 1).start()
-
         if with_dw and turn == 2:
             @pl.when((z >= 1) & first)
             def _():
@@ -376,6 +377,9 @@
             drain(xbuf.at[0, 0:3 * tok], x_r.at[k, 1])
             drain(xbuf.at[0, 0:2 * tok], x_r.at[k, 2])
 
+        wide = grp * DH // 2
+        chunks = list(range(2 * kvh))
+
         def w_copy(h, i, slot, to):
             return pltpu.make_async_remote_copy(
                 src_ref=part.at[h, i], dst_ref=precv.at[h, slot],
@@ -386,7 +390,7 @@
             w_copy(h, 1, slot, near).wait_recv()
 
         def send_part(h, i, slot, block, to, add=None):
-            new = dot(xt[block], dqall[h], NN)
+            new = dot(xt[block], dqall[h // 2, :, (h % 2) * wide:(h % 2 + 1) * wide], NN)
             if add is not None:
                 w_arrive(h, add)
                 new = new + precv[h, add].astype(F32)
@@ -417,14 +421,16 @@
             drain(dqall.at[h, 0:2 * tok], a_r.at[h, 0])
             @pl.when(outer)
             def _():
-                send_part(h, 0, 0, to_outer, near)
+                for each in (2 * h, 2 * h + 1):
+                    send_part(each, 0, 0, to_outer, near)
                 if h:
-                    for each in range(kvh):
+                    for each in chunks:
                         send_part(each, 2, 3, to_inner, near)
 
             @pl.when(inner)
             def _():
-                send_part(h, 1, 1, near, near)
+                for each in (2 * h, 2 * h + 1):
+                    send_part(each, 1, 1, near, near)
 
         @pl.when(w >= 2)
         def _():
@@ -432,14 +438,14 @@
 
         @pl.when(outer)
         def _():
-            for h in range(kvh):
-                send_part(h, 1, 1, near, near)
+            for each in chunks:
+                send_part(each, 1, 1, near, near)
 
         @pl.when(inner)
         def _():
-            for h in range(kvh):
+            for h in chunks:
                 send_part(h, 0, 2, to_outer, to_outer, 0)
-            for h in range(kvh):
+            for h in chunks:
                 send_part(h, 2, 2, to_inner, to_inner, 3)
 
         width = grp * DH
@@ -502,8 +508,8 @@
     dk_out[...] = acc[0].astype(BF)
     dv_out[...] = acc[1].astype(BF)
     if with_dw:
-        for h in range(kvh):
-            lanes = slice(h * width, (h + 1) * width)
+        for h in chunks:
+            lanes = slice(h * wide, (h + 1) * wide)
             w_arrive(h, 1)
             w_arrive(h, 2)
             dw_out[:, lanes] = dw_out[:, lanes] + precv[h, 1].astype(F32) + precv[h, 2].astype(F32)
@@ -568,14 +574,14 @@
             pltpu.VMEM((zn, wn * tok, rows), BF),
             pltpu.VMEM((zn, rows, wn * tok), BF),
             pltpu.VMEM((kvh, wn * tok, qw // kvh), BF),
-            pltpu.VMEM((kvh, zn - 1, rows, qw // kvh), BF),
-            pltpu.VMEM((kvh, zn, rows, qw // kvh), BF),
+            pltpu.VMEM((2 * kvh, zn - 1, rows, qw // kvh // 2), BF),
+            pltpu.VMEM((2 * kvh, zn, rows, qw // kvh // 2), BF),
             pltpu.SemaphoreType.DMA((2,)),
             pltpu.SemaphoreType.DMA((zper, 3)),
             pltpu.SemaphoreType.DMA,
             pltpu.SemaphoreType.DMA((kvh, 2)),
             pltpu.SemaphoreType.DMA,
-            pltpu.SemaphoreType.DMA((kvh, zn)),
+            pltpu.SemaphoreType.DMA((2 * kvh, zn)),
         ]
     outs = pl.pallas_call(
         functools.partial(kernel, (n, tp, with_dw)),

time: 30.4 us -> 29.7 us (0.977)
  Pallas kernels: 29.6 us -> 28.9 us
    pallas_call x1, Pallas kernels: 28.8 us -> 28.1 us  [shards(): pl.pallas_call(functools.partial(kernel, (n, tp, with_dw)), out_shape=[pl...]
where the time goes in v6:
time: 29.7 us; the launch traced here: 29.6 us
  Pallas kernels  28.9 us (97%)
  between operations  0.64 us (2%)
    pallas_call x1, Pallas kernels, shards(): pl.pallas_call(functools.partial(kernel, (n, tp, with_dw)), out_shape=[pl...  28.1 us
    pallas_call x1, Pallas kernels, shards(): pl.pallas_call(writer, out_shape=out_shape, in_specs=[vm] * len(out_shape...  0.84 us

profile of v6, /device:TPU:9, one launch (start us, length us, event | category | flops | bytes accessed | tf_op | source)
XLA Modules:
  0.0 29.6 jit_solution(6063450358138928676)
XLA Ops:
  0.6 28.1 %shard_map.111 = (bf16[192,512]{1,0:T(8,128)(2,1)S(1)}, bf16[192,128]{1,0:T(8,128)(2,1)S(1)}, bf16[192,128]{1,0:T(8,128)(2,1)S(1)}, f32[128,512]{1,0:T(8,128)S(1)}) custom-call(bf16[192,128]{1,0:T(8,128)(2,1)} %refs_0_.1, bf16[192,128]{1,0:T(8,128)(2,1)} %refs_1_.1, bf16[192,512]{1,0:T(8,128)(2,1)} %refs_2_.1, bf16[192,512]{1,0:T(8,128)(2,1)} %refs_3_.1, ...), custom_call_target="tpu_custom_call" | custom-call | tf_op jit(solution)/shard_map/pallas_call | solution.py:586
  28.7 0.8 %shard_map.112 = (bf16[192,512]{1,0:T(8,128)(2,1)}, bf16[192,128]{1,0:T(8,128)(2,1)}, bf16[192,128]{1,0:T(8,128)(2,1)}, f32[128,512]{1,0:T(8,128)}) custom-call(bf16[192,512]{1,0:T(8,128)(2,1)S(1)} %get-tuple-element.8.refs_0_, bf16[192,128]{1,0:T(8,128)(2,1)S(1)} %get-tuple-element.9.refs_1_, bf16[192,128]{1,0:T(8,128)(2,1)S(1)} %get-tuple-element.10.refs_2_, ...), custom_call_target="tpu_custom_call" | custom-call | tf_op jit(solution)/shard_map/pallas_call | solution.py:595

commit v7 on v6

--- a/solution.py
+++ b/solution.py
@@ -335,8 +335,8 @@
             far_pass(last, [h], picks(last))
         whole = (dqt[h] * scale).astype(BF)
         step = 2 if grp % 2 == 0 else 1
-        for qb in range(nb):
-            for g in range(0, grp, step):
+        for g in range(0, grp, step):
+            for qb in range(nb):
                 at = qb * part_cols + g * BLOCK
                 low = jnp.concatenate(
                     [whole[:, at + j * BLOCK:at + (j + 1) * BLOCK] for j in range(step)], axis=0).T
@@ -344,11 +344,12 @@
                 dq_out[qb * BLOCK:(qb + 1) * BLOCK, i * DH:(i + step) * DH] = low
                 if with_dw:
                     at_rows = pl.ds(pl.multiple_of(w * tok + qb * BLOCK, BLOCK), BLOCK)
-                    dqall[h, at_rows, g * DH:(g + step) * DH] = low
-        if with_dw:
-            for s in hops:
-                a_copy(h, s).start()
-            a_copy(h, 0).start()
+                    dqall[2 * h + g // 2, at_rows, g % 2 * DH:(g % 2 + step) * DH] = low
+            if with_dw and (g + step) % 2 == 0:
+                each = 2 * h + g // 2
+                for s in hops:
+                    a_copy(each, s).start()
+                a_copy(each, 0).start()
 
     @pl.when(me >= span(last))
     def _():
@@ -390,7 +391,7 @@
             w_copy(h, 1, slot, near).wait_recv()
 
         def send_part(h, i, slot, block, to, add=None):
-            new = dot(xt[block], dqall[h // 2, :, (h % 2) * wide:(h % 2 + 1) * wide], NN)
+            new = dot(xt[block], dqall[h], NN)
             if add is not None:
                 w_arrive(h, add)
                 new = new + precv[h, add].astype(F32)
@@ -404,25 +405,32 @@
 
         for h in range(kvh):
             if h == 0:
-                across_on(h)
+                across_on(0)
+                across_on(1)
 
                 @pl.when(second)
                 def _():
-                    for later in range(1, kvh):
-                        across_on(later)
+                    for each in chunks[2:]:
+                        across_on(each)
             else:
                 @pl.when(first)
                 def _():
-                    across_on(h)
+                    across_on(2 * h)
+                    across_on(2 * h + 1)
+
             if h < zper:
                 x_arrive(h)
                 for zz in ((lax.rem(near + 2, zn), near), (far, z))[h]:
                     xt[zz] = xbuf[zz].T
-            drain(dqall.at[h, 0:2 * tok], a_r.at[h, 0])
+            for each in (2 * h, 2 * h + 1):
+                drain(dqall.at[each, 0:2 * tok], a_r.at[each, 0])
+
+                @pl.when(outer)
+                def _():
+                    send_part(each, 0, 0, to_outer, near)
+
             @pl.when(outer)
             def _():
-                for each in (2 * h, 2 * h + 1):
-                    send_part(each, 0, 0, to_outer, near)
                 if h:
                     for each in chunks:
                         send_part(each, 2, 3, to_inner, near)
@@ -448,9 +456,8 @@
             for h in chunks:
                 send_part(h, 2, 2, to_inner, to_inner, 3)
 
-        width = grp * DH
-        for h in range(kvh):
-            dw_out[:, h * width:(h + 1) * width] = dot(xt[z], dqall[h], NN)
+        for h in chunks:
+            dw_out[:, h * wide:(h + 1) * wide] = dot(xt[z], dqall[h], NN)
         drain(xbuf.at[0:2], x_s.at[0])
         drain(xbuf.at[0:3, 0:2 * tok], x_s.at[1])
         drain(dqall.at[:, 0:3 * tok], a_s)
@@ -573,13 +580,13 @@
         scratch += [
             pltpu.VMEM((zn, wn * tok, rows), BF),
             pltpu.VMEM((zn, rows, wn * tok), BF),
-            pltpu.VMEM((kvh, wn * tok, qw // kvh), BF),
+            pltpu.VMEM((2 * kvh, wn * tok, qw // kvh // 2), BF),
             pltpu.VMEM((2 * kvh, zn - 1, rows, qw // kvh // 2), BF),
             pltpu.VMEM((2 * kvh, zn, rows, qw // kvh // 2), BF),
             pltpu.SemaphoreType.DMA((2,)),
             pltpu.SemaphoreType.DMA((zper, 3)),
             pltpu.SemaphoreType.DMA,
-            pltpu.SemaphoreType.DMA((kvh, 2)),
+            pltpu.SemaphoreType.DMA((2 * kvh, 2)),
             pltpu.SemaphoreType.DMA,
             pltpu.SemaphoreType.DMA((2 * kvh, zn)),
         ]

time: 29.7 us -> 29.6 us (level)
  the two profiles are of different devices: /device:TPU:9 before, /device:TPU:0 now
where the time goes in v7:
time: 29.6 us; the launch traced here: 29.3 us
  Pallas kernels  28.6 us (97%)
  between operations  0.64 us (2%)
    pallas_call x1, Pallas kernels, shards(): pl.pallas_call(functools.partial(kernel, (n, tp, with_dw)), out_shape=[pl...  27.8 us
    pallas_call x1, Pallas kernels, shards(): pl.pallas_call(writer, out_shape=out_shape, in_specs=[vm] * len(out_shape...  0.84 us

profile of v7, /device:TPU:0, one launch (start us, length us, event | category | flops | bytes accessed | tf_op | source)
XLA Modules:
  0.0 29.3 jit_solution(4175465069006857928)
XLA Ops:
  0.6 27.8 %shard_map.111 = (bf16[192,512]{1,0:T(8,128)(2,1)S(1)}, bf16[192,128]{1,0:T(8,128)(2,1)S(1)}, bf16[192,128]{1,0:T(8,128)(2,1)S(1)}, f32[128,512]{1,0:T(8,128)S(1)}) custom-call(bf16[192,128]{1,0:T(8,128)(2,1)} %refs_0_.1, bf16[192,128]{1,0:T(8,128)(2,1)} %refs_1_.1, bf16[192,512]{1,0:T(8,128)(2,1)} %refs_2_.1, bf16[192,512]{1,0:T(8,128)(2,1)} %refs_3_.1, ...), custom_call_target="tpu_custom_call" | custom-call | tf_op jit(solution)/shard_map/pallas_call | solution.py:593
  28.4 0.8 %shard_map.112 = (bf16[192,512]{1,0:T(8,128)(2,1)}, bf16[192,128]{1,0:T(8,128)(2,1)}, bf16[192,128]{1,0:T(8,128)(2,1)}, f32[128,512]{1,0:T(8,128)}) custom-call(bf16[192,512]{1,0:T(8,128)(2,1)S(1)} %get-tuple-element.8.refs_0_, bf16[192,128]{1,0:T(8,128)(2,1)S(1)} %get-tuple-element.9.refs_1_, bf16[192,128]{1,0:T(8,128)(2,1)S(1)} %get-tuple-element.10.refs_2_, ...), custom_call_target="tpu_custom_call" | custom-call | tf_op jit(solution)/shard_map/pallas_call | solution.py:602

commit v8 on v7

--- a/solution.py
+++ b/solution.py
@@ -43,7 +43,7 @@
     q_ref, g_ref, o_ref = qgo.at[0], qgo.at[1], qgo.at[2]
     if with_dw:
         dw_out = outs[3]
-        (xbuf, xt, dqall, part, precv, x_s, x_r, a_s, a_r, w_s, w_r) = refs[14:]
+        (xbuf, xt, dqall, part, precv, x_s, x_r, a_s, a_r, w_s, w_r, w_n) = refs[14:]
     places = [k_ref, v_ref, q_ref, g_ref, o_ref, lse_ref] + ([x_ref] if with_dw else [])
     for i, to in enumerate(places):
         pltpu.make_async_copy(hbm[i], to, in_s.at[(0, 0, 1, 1, 1, 2, 4)[i]]).start()
@@ -384,7 +384,7 @@
         def w_copy(h, i, slot, to):
             return pltpu.make_async_remote_copy(
                 src_ref=part.at[h, i], dst_ref=precv.at[h, slot],
-                send_sem=w_s, recv_sem=w_r.at[h, slot],
+                send_sem=w_s, recv_sem=w_n if slot == 1 else w_r.at[h, max(slot - 1, 0)],
                 device_id={"kv": to * wn + w}, device_id_type=pl.DeviceIdType.MESH)
 
         def w_arrive(h, slot):
@@ -517,7 +517,8 @@
     if with_dw:
         for h in chunks:
             lanes = slice(h * wide, (h + 1) * wide)
-            w_arrive(h, 1)
+            if h == 0:
+                drain(precv.at[:, 1], w_n)
             w_arrive(h, 2)
             dw_out[:, lanes] = dw_out[:, lanes] + precv[h, 1].astype(F32) + precv[h, 2].astype(F32)
         drain(part, w_s)
@@ -588,7 +589,8 @@
             pltpu.SemaphoreType.DMA,
             pltpu.SemaphoreType.DMA((2 * kvh, 2)),
             pltpu.SemaphoreType.DMA,
-            pltpu.SemaphoreType.DMA((2 * kvh, zn)),
+            pltpu.SemaphoreType.DMA((2 * kvh, zn - 1)),
+            pltpu.SemaphoreType.DMA,
         ]
     outs = pl.pallas_call(
         functools.partial(kernel, (n, tp, with_dw)),

time: 29.6 us -> 29.5 us (level)
  no operation moved by 1% of the time
where the time goes in v8:
time: 29.5 us; the launch traced here: 29.2 us
  Pallas kernels  28.6 us (97%)
  between operations  0.64 us (2%)
    pallas_call x1, Pallas kernels, shards(): pl.pallas_call(functools.partial(kernel, (n, tp, with_dw)), out_shape=[pl...  27.8 us
    pallas_call x1, Pallas kernels, shards(): pl.pallas_call(writer, out_shape=out_shape, in_specs=[vm] * len(out_shape...  0.84 us

profile of v8, /device:TPU:0, one launch (start us, length us, event | category | flops | bytes accessed | tf_op | source)
XLA Modules:
  0.0 29.2 jit_solution(3177515332450304842)
XLA Ops:
  0.6 27.8 %shard_map.111 = (bf16[192,512]{1,0:T(8,128)(2,1)S(1)}, bf16[192,128]{1,0:T(8,128)(2,1)S(1)}, bf16[192,128]{1,0:T(8,128)(2,1)S(1)}, f32[128,512]{1,0:T(8,128)S(1)}) custom-call(bf16[192,128]{1,0:T(8,128)(2,1)} %refs_0_.1, bf16[192,128]{1,0:T(8,128)(2,1)} %refs_1_.1, bf16[192,512]{1,0:T(8,128)(2,1)} %refs_2_.1, bf16[192,512]{1,0:T(8,128)(2,1)} %refs_3_.1, ...), custom_call_target="tpu_custom_call" | custom-call | tf_op jit(solution)/shard_map/pallas_call | solution.py:595
  28.4 0.8 %shard_map.112 = (bf16[192,512]{1,0:T(8,128)(2,1)}, bf16[192,128]{1,0:T(8,128)(2,1)}, bf16[192,128]{1,0:T(8,128)(2,1)}, f32[128,512]{1,0:T(8,128)}) custom-call(bf16[192,512]{1,0:T(8,128)(2,1)S(1)} %get-tuple-element.8.refs_0_, bf16[192,128]{1,0:T(8,128)(2,1)S(1)} %get-tuple-element.9.refs_1_, bf16[192,128]{1,0:T(8,128)(2,1)S(1)} %get-tuple-element.10.refs_2_, ...), custom_call_target="tpu_custom_call" | custom-call | tf_op jit(solution)/shard_map/pallas_call | solution.py:604
